TPU v7x, 32 devices: a whole 2x2x4 slice. The times are simulated.
32 devices in a mesh: grp: 2 (over x), ep: 4 (over y, core), tp: 4 (over z).
Axes of the slice: x: 2, y: 2, z: 4, core: 2. Of those that a mesh axis runs over, the one named last changes fastest.
Arguments:
- tokens: bfloat16 [4096, 1024], P(('grp', 'ep', 'tp')), parts along dimension 0, may hold values from -6 to 6
- norm_gain: float32 [1024], replicated, may hold values from 0.1 to 1.9
- gate_weight: bfloat16 [4, 1024, 3584], P('ep', None, 'tp'), may hold values from -0.1875 to 0.1875
- up_weight: bfloat16 [4, 1024, 3584], P('ep', None, 'tp'), may hold values from -0.1875 to 0.1875
- down_weight: bfloat16 [4, 3584, 1024], P('ep', 'tp'), may hold values from -0.09375 to 0.09375
- expert_ids: int32 [4096, 2], P(('grp', 'ep')), parts along dimension 0, may hold values from 0 to 3, all different within a row; in each aligned block of 128 rows (0 to 127, 128 to 255, ...) at most 80 rows name the same one
- route_weight: float32 [4096, 2], P(('grp', 'ep')), parts along dimension 0, may hold values from 0.2 to 1
Outputs:
- mixed: bfloat16 [4096, 1024], P(('grp', 'ep', 'tp')), parts along dimension 0
There are 2 independent parts, one for each index of `grp`. A program takes and returns all parts, laid end to end along the dimension named above; an argument that names none is the same for every part. Nothing has to cross between parts.
Inputs may be any that keep to these rules, and one draw needn't show every extreme that they name: `expert_ids`: A token's 2 experts differ. In the rows of one device (128 tokens, aligned blocks) no expert is named more than 80 times, and in every draw some expert is named exactly 80 times in some device's rows.
All inputs are finite; a program needn't handle non-finite values.
Results may differ from a plain program's by a relative error of at most 0.015.
Values may be sent and summed in bfloat16 or wider, within the bound.
A program may use at most 64 MiB of HBM per device.

v0:
```python
import functools

import jax
import jax.numpy as jnp
from jax import lax
from jax.experimental import pallas as pl
from jax.experimental.pallas import tpu as pltpu
from jax.sharding import PartitionSpec as P

TOP_K = 2
MESH = pl.DeviceIdType.MESH
VMEM_ROOM = 60 << 20


def norm_rows(tokens, norm_gain):
    values = tokens.astype(jnp.float32)
    scaled = values * lax.rsqrt(jnp.mean(values * values, axis=-1, keepdims=True) + 1e-06)
    return (scaled * norm_gain).astype(jnp.bfloat16)


def expert_hidden(rows, gate_weight, up_weight):
    gate = jnp.einsum("e...d,edf->e...f", rows, gate_weight, preferred_element_type=jnp.float32)
    upper = jnp.einsum("e...d,edf->e...f", rows, up_weight, preferred_element_type=jnp.float32)
    return (jax.nn.silu(gate) * upper).astype(jnp.bfloat16)


def weigh_pieces(summed, weights):
    piece = lax.optimization_barrier(summed.astype(jnp.bfloat16)).astype(jnp.float32)
    total = piece[:, 0] * weights[:, 0:1]
    total = total + piece[:, 1] * weights[:, 1:2]
    return total.astype(jnp.bfloat16)


def plain_body(tokens, norm_gain, gate_weight, up_weight, down_weight, expert_ids, route_weight):
    tok_rows = tokens.shape[0]
    width = tokens.shape[1]
    local_experts = gate_weight.shape[0]
    inner = gate_weight.shape[2]
    n_tp = lax.axis_size("tp")
    n_ep = lax.axis_size("ep")
    experts = n_ep * local_experts
    most = max(2, tok_rows * TOP_K * 5 // (4 * experts))
    normed = norm_rows(tokens, norm_gain)
    flat_ids = expert_ids.reshape(n_tp, tok_rows * TOP_K)
    onehot = (flat_ids[:, :, None] == jnp.arange(experts, dtype=jnp.int32)[None, None, :]).astype(
        jnp.int32
    )
    before = jnp.cumsum(onehot, axis=1) - onehot
    slots = jnp.sum(before * onehot, axis=-1)
    owner = jnp.arange(n_tp, dtype=jnp.int32)[:, None]
    row_index = (flat_ids * (n_tp * most) + owner * most + slots).reshape(-1)
    mine = lax.axis_index("tp")
    own_ids = lax.dynamic_slice_in_dim(flat_ids, mine, 1, 0)[0]
    own_slots = lax.dynamic_slice_in_dim(slots, mine, 1, 0)[0]
    own_index = own_ids * most + own_slots
    whole = lax.all_gather(normed, "tp", axis=0, tiled=True)
    sending = (
        jnp.zeros((experts * n_tp * most, width), jnp.bfloat16)
        .at[row_index]
        .set(jnp.repeat(whole, TOP_K, axis=0))
    )
    arrived = lax.all_to_all(
        sending.reshape(experts, n_tp * most, width), "ep", split_axis=0, concat_axis=1, tiled=True
    )
    hidden = expert_hidden(arrived, gate_weight, up_weight)
    by_source = hidden.reshape(local_experts, n_ep, n_tp, most, inner).transpose(2, 0, 1, 3, 4)
    per_device = local_experts * n_ep * most
    product = jnp.einsum(
        "tlnmf,lfd->tlnmd", by_source, down_weight, preferred_element_type=jnp.float32
    )
    own_sums = lax.psum_scatter(
        product.astype(jnp.bfloat16)
        .astype(jnp.float32)
        .reshape(per_device * lax.axis_size("tp"), width)
        .astype(jnp.bfloat16),
        "tp",
        scatter_dimension=0,
        tiled=True,
    )
    own_pieces = own_sums.reshape(local_experts, n_ep, most, width)
    back = lax.all_to_all(own_pieces, "ep", split_axis=1, concat_axis=0, tiled=True)
    picked = back.reshape(experts * most, width)[own_index].reshape(tok_rows, TOP_K, width)
    own_weights = lax.dynamic_slice_in_dim(route_weight, mine * tok_rows, tok_rows, 0)
    return weigh_pieces(picked.astype(jnp.float32), own_weights)


def place(step, n):
    last = step // (2 * n - 1)
    later = (step + 2 * n - 2) // (2 * n - 1)
    dy = ((step + 1) % 2) * later + last
    dz = (1 - dy) * ((step + 1) // 2) + dy * (step // 2 - 1 + last)
    return dy, dz


def step_of(dy, dz, n):
    if dy == 0:
        return 2 * dz - 1 if dz else 0
    return 2 * n - 1 if dz == n - 1 else 2 * dz + 2


def kernel(
    n, tok_ref, gain_ref, share_ref, gate_hbm, up_hbm, down_hbm, out_ref,
    gate, up, down, buf, shares, part, srecv, yrecv, zrecv, tbuf,
    load_sem, w_s, w_r, agz_s, agz_r, agy_s, agy_r, ags_s, ags_r, rss_s, rss_r, rsy_s, rsy_r, rsz_s, rsz_r,
):
    ep = lax.axis_index("ep")
    z = lax.axis_index("tp")
    y, c = ep // 2, ep % 2
    rows, width = tok_ref.shape
    steps = 2 * n
    sib = {"ep": 2 * y + 1 - c}
    across = {"ep": 2 * (1 - y) + c}

    def along(k):
        return {"tp": (z + k) % n}

    def remote(src, dst, send, recv, to):
        return pltpu.make_async_remote_copy(
            src_ref=src, dst_ref=dst, send_sem=send, recv_sem=recv, device_id=to, device_id_type=MESH
        )

    loads = [
        pltpu.make_async_copy(src.at[0], dst, load_sem.at[i])
        for i, (src, dst) in enumerate(((gate_hbm, gate), (up_hbm, up), (down_hbm, down)))
    ]
    for load in loads:
        load.start()

    barrier = pltpu.get_barrier_semaphore()
    for k in range(1, 4):
        pl.semaphore_signal(barrier, inc=1, device_id={"ep": (ep + k) % 4}, device_id_type=MESH)
    for k in range(1, n):
        pl.semaphore_signal(barrier, inc=1, device_id=along(k), device_id_type=MESH)
    buf[z, y, c] = norm_rows(tok_ref[...], gain_ref[...])
    pl.semaphore_wait(barrier, 3 + n - 1)

    def ag_sib(step):
        dy, dz = place(step, n)
        yb, zb = (y + dy) % 2, (z + dz) % n
        return remote(buf.at[zb, yb, c], buf.at[zb, yb, c], ags_s.at[step], ags_r.at[step], sib)

    def ag_y(dz):
        zb = (z + dz) % n
        return remote(buf.at[zb, y, c], buf.at[zb, y, c], agy_s.at[dz], agy_r.at[dz], across)

    def ag_z(k):
        return remote(buf.at[z, y, c], buf.at[z, y, c], agz_s.at[k], agz_r.at[n - k], along(k))

    def share(k):
        to = (ep + k) % 4
        return remote(share_ref.at[to], shares.at[ep], w_s.at[k], w_r.at[4 - k], {"ep": to})

    def rs_sib(step):
        return remote(part.at[step, 1 - c], srecv.at[step], rss_s.at[step], rss_r.at[step], sib)

    def rs_y(dz, step):
        return remote(part.at[step, c], yrecv.at[dz], rsy_s.at[dz], rsy_r.at[dz], across)

    def rs_z(dz):
        return remote(tbuf.at[dz - 1], zrecv.at[n - dz - 1], rsz_s.at[dz], rsz_r.at[n - dz], along(dz))

    ag_y(0).start()
    for k in reversed(range(1, n)):
        ag_z(k).start()
    for k in range(1, 4):
        share(k).start()
    shares[ep] = share_ref[ep]
    for k in range(1, 4):
        remote(share_ref.at[0], shares.at[(ep + k) % 4], w_s.at[k], w_r.at[k], sib).wait_recv()
    for load in loads:
        load.wait()

    def arrive(step):
        dy, dz = place(step, n)
        yb, zb = (y + dy) % 2, (z + dz) % n
        here = buf.at[zb, yb, c]

        @pl.when(dy == 1)
        def _():
            remote(here, here, agy_s.at[dz], agy_r.at[dz], across).wait_recv()

        @pl.when((dy == 0) & (dz > 0))
        def _():
            remote(here, here, agz_s.at[dz], agz_r.at[dz], sib).wait_recv()
            ag_y(dz).start()

        ag_sib(step).start()

    def combine(step):
        dy, dz = place(step, n)
        rs_sib(step).wait_recv()
        part[step, c] = (part[step, c].astype(jnp.float32) + srecv[step].astype(jnp.float32)).astype(jnp.bfloat16)

        @pl.when((dy == 1) & (dz > 0))
        def _():
            rs_y(dz, step).start()

    def column(row):
        return jnp.transpose(jnp.broadcast_to(row, (rows, rows)))[:, :1]

    def one(step, carry):
        dy, dz = place(step, n)
        yb, zb = (y + dy) % 2, (z + dz) % n
        arrive(step)
        theirs = buf.at[zb, yb, 1 - c]
        remote(theirs, theirs, ags_s.at[step], ags_r.at[step], sib).wait_recv()
        x = buf[zb, yb].reshape(2 * rows, width)
        g = jnp.dot(x, gate[...], preferred_element_type=jnp.float32)
        u = jnp.dot(x, up[...], preferred_element_type=jnp.float32)
        hidden = (jax.nn.silu(g) * u).astype(jnp.bfloat16)
        product = jnp.dot(hidden, down[...], preferred_element_type=jnp.float32)
        for half in range(2):
            w = column(shares[2 * yb + half, pl.ds(zb, 1), :])
            part[step, half] = (product[half * rows : (half + 1) * rows] * w).astype(jnp.bfloat16)
        rs_sib(step).start()

        @pl.when(step > 0)
        def _():
            combine(step - 1)

        return carry

    lax.fori_loop(0, steps, one, 0)
    combine(steps - 1)
    rs_y(0, step_of(1, 0, n)).start()

    def total(dz):
        landed = yrecv.at[dz]
        remote(landed, landed, rsy_s.at[dz], rsy_r.at[dz], across).wait_recv()
        return part[step_of(0, dz, n), c].astype(jnp.float32) + yrecv[dz].astype(jnp.float32)

    for dz in range(1, n):
        tbuf[dz - 1] = total(dz).astype(jnp.bfloat16)
        rs_z(dz).start()
    result = total(0)
    for dz in range(1, n):
        landed = zrecv.at[dz - 1]
        remote(landed, landed, rsz_s.at[dz], rsz_r.at[dz], sib).wait_recv()
        result = result + zrecv[dz - 1].astype(jnp.float32)
    out_ref[...] = result.astype(out_ref.dtype)

    for k in range(1, 4):
        share(k).wait_send()
    for k in range(1, n):
        ag_z(k).wait_send()
        rs_z(k).wait_send()
    for dz in range(n):
        ag_y(dz).wait_send()
        rs_y(dz, step_of(1, dz, n)).wait_send()
    for step in range(steps):
        ag_sib(step).wait_send()
        rs_sib(step).wait_send()


def kernel_bytes(n, rows, width, inner):
    blocks = n * 4 + 2 * n * 2 + 2 * n + n + 2 * (n - 1) + 8
    return 2 * width * (3 * inner + blocks * rows) + 16 * rows * (width + 2 * inner)


def fused_body(tokens, norm_gain, gate_weight, up_weight, down_weight, expert_ids, route_weight):
    rows, width = tokens.shape
    inner = gate_weight.shape[2]
    n = lax.axis_size("tp")
    experts = lax.axis_size("ep")
    named = expert_ids[None, :, :] == jnp.arange(experts, dtype=jnp.int32)[:, None, None]
    share = jnp.sum(jnp.where(named, route_weight[None, :, :], 0.0), axis=-1).reshape(experts, n, rows)
    vmem = pl.BlockSpec(memory_space=pltpu.VMEM)
    anywhere = pl.BlockSpec(memory_space=pl.ANY)
    dma = pltpu.SemaphoreType.DMA
    bf16 = jnp.bfloat16
    return pl.pallas_call(
        functools.partial(kernel, n),
        out_shape=jax.ShapeDtypeStruct((rows, width), bf16),
        in_specs=[vmem] * 3 + [anywhere] * 3,
        out_specs=vmem,
        scratch_shapes=[
            pltpu.VMEM((width, inner), bf16),
            pltpu.VMEM((width, inner), bf16),
            pltpu.VMEM((inner, width), bf16),
            pltpu.VMEM((n, 2, 2, rows, width), bf16),
            pltpu.VMEM((experts, n, rows), jnp.float32),
            pltpu.VMEM((2 * n, 2, rows, width), bf16),
            pltpu.VMEM((2 * n, rows, width), bf16),
            pltpu.VMEM((n, rows, width), bf16),
            pltpu.VMEM((n - 1, rows, width), bf16),
            pltpu.VMEM((n - 1, rows, width), bf16),
            dma((3,)),
        ]
        + [dma((4,))] * 2
        + [dma((n,))] * 4
        + [dma((2 * n,))] * 4
        + [dma((n,))] * 4,
        compiler_params=pltpu.CompilerParams(
            collective_id=0, has_side_effects=True, vmem_limit_bytes=VMEM_ROOM
        ),
    )(tokens, norm_gain.reshape(1, width), share, gate_weight, up_weight, down_weight)


def body(tokens, norm_gain, gate_weight, up_weight, down_weight, expert_ids, route_weight):
    rows, width = tokens.shape
    inner = gate_weight.shape[2]
    n = lax.axis_size("tp")
    fits = kernel_bytes(n, rows, width, inner) <= VMEM_ROOM
    chosen = plain_body
    if lax.axis_size("ep") == 4 and gate_weight.shape[0] == 1 and n > 1 and fits:
        chosen = fused_body
    return chosen(tokens, norm_gain, gate_weight, up_weight, down_weight, expert_ids, route_weight)


def solution(mesh):
    placed = (
        P(("grp", "ep", "tp"), None),
        P(),
        P("ep", None, "tp"),
        P("ep", None, "tp"),
        P("ep", "tp", None),
        P(("grp", "ep"), None),
        P(("grp", "ep"), None),
    )
    return jax.shard_map(
        body, mesh=mesh, in_specs=placed, out_specs=P(("grp", "ep", "tp"), None), check_vma=False
    )
```

profile of v0, /device:TPU:25, one launch (start us, length us, event | category | flops | bytes accessed | tf_op | source)
XLA Modules:
  0.0 76.2 jit_solution(6991520795850281403)
XLA Ops:
  0.0 0.7 select_reduce_fusion
  0.7 0.6 reshape.9.share_ref
  1.3 73.1 %shard_map.73 = bf16[128,1024]{1,0:T(8,128)(2,1)} custom-call(bf16[128,1024]{1,0:T(8,128)(2,1)} %tok_ref.1, f32[1,1024]{1,0:T(1,128)} %bitcast.1, f32[4,4,128]{2,1,0:T(4,128)} %reshape.9.share_ref, bf16[1,1024,896]{2,1,0:T(8,128)(2,1)} %gate_hbm.1, bf16[1,1024,896]{2,1,0:T(8,128)(2,1)} %up_hbm.1, bf16[1,896,1024]{2,1,0:T(8,128)(2,1)} %down_hbm.1), custom_call_target="tpu_custom_call" | custom-call | tf_op jit(solution)/shard_map/pallas_call | solution.py:271
  74.5 1.7 %copy.11 = bf16[128,1024]{1,0:T(8,128)(2,1)} copy(bf16[128,1024]{1,0:T(8,128)(2,1)} %shard_map.73) | data formatting | bytes 524288
where the time goes:
time: 76.4 us; the launch traced here: 76.2 us
  Pallas kernels  73.1 us (96%)
  local copies, waits for them, and re-layouts  2.28 us (3%)
    pallas_call x1, Pallas kernels, fused_body(): pl.pallas_call(functools.partial(kernel, n), out_shape=jax.ShapeDtypeStru...  73.1 us
    unnamed x1, local copies, waits for them, and re-layouts  1.67 us

commit v1 on v0

v1 whole, which is shorter than its diff:
```python
import functools

import jax
import jax.numpy as jnp
from jax import lax
from jax.experimental import pallas as pl
from jax.experimental.pallas import tpu as pltpu
from jax.sharding import PartitionSpec as P

TOP_K = 2
MESH = pl.DeviceIdType.MESH
VMEM_ROOM = 60 << 20

ACROSS, INWARD, OUTWARD = range(3)
RELAY, SEND, REDUCE, COMPUTE = range(4)
UNITS = 2
PIECES = 4
LINE = 4
CROSSES = ((True, True, False, False), (True, True, True, False))
ORDER = (
    (
        (0, 0, 0, 0, 0), (0, 0, 0, 1, 0), (0, 0, 0, 2, 0), (0, 0, 0, 3, 0), (1, 0, 0, 1, 1), (1, 0, 0, 0, 0),
        (1, 0, 0, 2, 1), (1, 0, 0, 1, 0), (3, 0, 0, 1, 0), (1, 0, 0, 0, 1), (1, 0, 0, 2, 0), (3, 0, 0, 0, 0),
        (0, 0, 1, 2, 0), (0, 1, 0, 0, 0), (1, 0, 0, 3, 1), (1, 0, 0, 3, 0), (1, 0, 1, 2, 0), (0, 1, 0, 1, 0),
        (0, 0, 1, 1, 0), (3, 1, 0, 0, 0), (0, 1, 0, 2, 0), (0, 0, 1, 3, 0), (1, 0, 1, 1, 0), (1, 1, 0, 2, 1),
        (0, 1, 0, 3, 0), (0, 0, 2, 1, 0), (1, 0, 2, 1, 0), (1, 1, 0, 3, 1), (3, 0, 1, 1, 0), (0, 1, 1, 2, 0),
        (0, 1, 1, 3, 0), (2, 1, 0, 1, 0), (3, 1, 0, 1, 0), (0, 0, 2, 2, 0), (0, 1, 1, 1, 0), (1, 0, 2, 2, 0),
        (2, 0, 1, 3, 1), (3, 1, 1, 1, 0), (0, 1, 2, 1, 0), (0, 1, 2, 3, 0), (2, 1, 0, 0, 0), (2, 1, 1, 2, 0),
        (2, 1, 1, 3, 1), (0, 0, 3, 1, 0), (1, 0, 3, 1, 0), (0, 1, 2, 2, 0), (0, 0, 3, 2, 0), (3, 1, 2, 1, 0),
        (0, 0, 3, 3, 0), (2, 0, 1, 2, 1), (0, 0, 3, 0, 0), (1, 0, 3, 0, 0), (3, 0, 3, 1, 0), (0, 1, 3, 1, 0),
        (0, 1, 3, 2, 0), (2, 1, 2, 2, 0), (2, 1, 2, 3, 1), (3, 0, 3, 0, 0), (0, 1, 3, 3, 0), (2, 0, 3, 2, 1),
        (0, 1, 3, 0, 0), (2, 0, 3, 3, 1), (3, 1, 3, 1, 0), (0, 0, 2, 0, 0), (1, 0, 2, 0, 0), (3, 1, 3, 0, 0),
        (0, 0, 2, 3, 0), (3, 0, 2, 0, 0), (0, 0, 1, 0, 0), (2, 1, 3, 2, 1), (2, 1, 3, 1, 0), (3, 0, 2, 1, 0),
        (0, 1, 2, 0, 0), (2, 1, 3, 3, 1), (1, 0, 1, 0, 0), (3, 0, 1, 0, 0), (2, 0, 2, 2, 1), (2, 1, 3, 0, 0),
        (3, 1, 2, 0, 0), (2, 0, 3, 1, 1), (2, 0, 2, 3, 1), (0, 1, 1, 0, 0), (2, 1, 2, 0, 0), (2, 1, 2, 1, 0),
        (3, 1, 1, 0, 0), (2, 0, 3, 0, 1), (2, 1, 1, 0, 0), (2, 0, 2, 0, 1), (2, 1, 1, 1, 0), (2, 0, 2, 1, 1),
        (2, 1, 0, 2, 0), (2, 1, 0, 3, 0), (2, 0, 1, 0, 1), (2, 0, 1, 1, 1), (2, 0, 0, 1, 0), (2, 0, 0, 2, 0),
        (2, 0, 0, 3, 0), (2, 0, 0, 0, 0),
    ),
    (
        (0, 0, 1, 0, 0), (0, 0, 1, 1, 0), (0, 0, 1, 2, 0), (0, 0, 1, 3, 0), (1, 0, 1, 1, 1), (1, 0, 1, 3, 0),
        (1, 0, 1, 2, 2), (1, 0, 1, 2, 1), (1, 0, 1, 0, 0), (1, 0, 1, 1, 2), (3, 0, 1, 1, 0), (1, 0, 1, 3, 1),
        (1, 0, 1, 2, 0), (1, 0, 1, 3, 2), (3, 0, 1, 0, 0), (0, 0, 0, 1, 0), (0, 0, 2, 1, 0), (0, 1, 1, 3, 0),
        (1, 1, 1, 3, 1), (1, 0, 2, 1, 2), (1, 0, 2, 1, 0), (1, 0, 0, 1, 1), (1, 0, 1, 1, 0), (1, 1, 1, 3, 2),
        (0, 0, 0, 2, 0), (0, 0, 2, 2, 0), (0, 1, 1, 0, 0), (1, 0, 0, 2, 1), (1, 0, 2, 2, 0), (1, 0, 2, 2, 2),
        (0, 0, 0, 0, 0), (0, 0, 2, 3, 0), (0, 1, 1, 2, 0), (3, 0, 0, 0, 0), (0, 0, 0, 3, 0), (0, 1, 2, 3, 0),
        (0, 1, 2, 1, 0), (1, 0, 0, 3, 1), (1, 0, 0, 0, 0), (1, 1, 2, 3, 2), (3, 1, 1, 1, 0), (0, 0, 3, 1, 0),
        (0, 1, 1, 1, 0), (1, 0, 0, 0, 1), (1, 0, 3, 1, 2), (1, 0, 3, 1, 0), (3, 0, 0, 1, 0), (0, 1, 0, 2, 0),
        (0, 0, 3, 2, 0), (0, 1, 2, 2, 0), (1, 1, 0, 2, 1), (2, 1, 1, 2, 0), (1, 0, 3, 2, 2), (3, 1, 1, 0, 0),
        (0, 1, 0, 3, 0), (0, 0, 3, 3, 0), (0, 1, 0, 0, 0), (1, 1, 0, 3, 1), (1, 0, 3, 3, 2), (1, 0, 0, 1, 0),
        (3, 0, 2, 1, 0), (0, 0, 3, 0, 0), (0, 1, 3, 1, 0), (2, 1, 1, 0, 0), (1, 0, 1, 0, 1), (1, 0, 3, 0, 2),
        (3, 0, 3, 1, 0), (0, 1, 3, 2, 0), (1, 1, 3, 2, 2), (1, 0, 3, 0, 0), (3, 0, 3, 0, 0), (0, 1, 3, 3, 0),
        (0, 1, 0, 1, 0), (1, 1, 3, 3, 2), (2, 1, 1, 1, 0), (3, 1, 2, 1, 0), (0, 0, 2, 0, 0), (1, 0, 2, 0, 0),
        (1, 0, 2, 0, 2), (3, 1, 0, 1, 0), (3, 0, 2, 0, 0), (0, 1, 3, 0, 0), (2, 1, 2, 2, 0), (1, 0, 2, 3, 2),
        (3, 1, 0, 0, 0), (1, 0, 1, 0, 2), (3, 1, 3, 0, 0), (0, 1, 2, 0, 0), (3, 1, 3, 1, 0), (2, 1, 2, 3, 1),
        (2, 1, 3, 0, 0), (3, 1, 2, 0, 0), (2, 0, 3, 2, 1), (2, 1, 3, 1, 0), (2, 1, 0, 0, 0), (2, 0, 3, 3, 1),
        (2, 1, 0, 1, 0), (2, 1, 2, 1, 0), (2, 0, 0, 2, 2), (2, 1, 3, 2, 1), (2, 1, 1, 3, 0), (2, 0, 0, 3, 2),
        (2, 1, 3, 3, 1), (2, 1, 2, 0, 0), (2, 0, 2, 2, 1), (2, 1, 0, 2, 2), (2, 0, 3, 1, 1), (2, 1, 0, 3, 2),
        (2, 0, 2, 3, 1), (2, 0, 1, 2, 0), (2, 0, 3, 0, 1), (2, 0, 0, 1, 2), (2, 0, 2, 0, 1), (2, 0, 1, 3, 0),
        (2, 0, 2, 1, 1), (2, 0, 0, 0, 2), (2, 0, 1, 0, 0), (2, 0, 1, 1, 0),
    ),
)


def norm_rows(tokens, norm_gain):
    values = tokens.astype(jnp.float32)
    scaled = values * lax.rsqrt(jnp.mean(values * values, axis=-1, keepdims=True) + 1e-06)
    return (scaled * norm_gain).astype(jnp.bfloat16)


def expert_hidden(rows, gate_weight, up_weight):
    gate = jnp.einsum("e...d,edf->e...f", rows, gate_weight, preferred_element_type=jnp.float32)
    upper = jnp.einsum("e...d,edf->e...f", rows, up_weight, preferred_element_type=jnp.float32)
    return (jax.nn.silu(gate) * upper).astype(jnp.bfloat16)


def weigh_pieces(summed, weights):
    piece = lax.optimization_barrier(summed.astype(jnp.bfloat16)).astype(jnp.float32)
    total = piece[:, 0] * weights[:, 0:1]
    total = total + piece[:, 1] * weights[:, 1:2]
    return total.astype(jnp.bfloat16)


def plain_body(tokens, norm_gain, gate_weight, up_weight, down_weight, expert_ids, route_weight):
    tok_rows = tokens.shape[0]
    width = tokens.shape[1]
    local_experts = gate_weight.shape[0]
    inner = gate_weight.shape[2]
    n_tp = lax.axis_size("tp")
    n_ep = lax.axis_size("ep")
    experts = n_ep * local_experts
    most = max(2, tok_rows * TOP_K * 5 // (4 * experts))
    normed = norm_rows(tokens, norm_gain)
    flat_ids = expert_ids.reshape(n_tp, tok_rows * TOP_K)
    onehot = (flat_ids[:, :, None] == jnp.arange(experts, dtype=jnp.int32)[None, None, :]).astype(
        jnp.int32
    )
    before = jnp.cumsum(onehot, axis=1) - onehot
    slots = jnp.sum(before * onehot, axis=-1)
    owner = jnp.arange(n_tp, dtype=jnp.int32)[:, None]
    row_index = (flat_ids * (n_tp * most) + owner * most + slots).reshape(-1)
    mine = lax.axis_index("tp")
    own_ids = lax.dynamic_slice_in_dim(flat_ids, mine, 1, 0)[0]
    own_slots = lax.dynamic_slice_in_dim(slots, mine, 1, 0)[0]
    own_index = own_ids * most + own_slots
    whole = lax.all_gather(normed, "tp", axis=0, tiled=True)
    sending = (
        jnp.zeros((experts * n_tp * most, width), jnp.bfloat16)
        .at[row_index]
        .set(jnp.repeat(whole, TOP_K, axis=0))
    )
    arrived = lax.all_to_all(
        sending.reshape(experts, n_tp * most, width), "ep", split_axis=0, concat_axis=1, tiled=True
    )
    hidden = expert_hidden(arrived, gate_weight, up_weight)
    by_source = hidden.reshape(local_experts, n_ep, n_tp, most, inner).transpose(2, 0, 1, 3, 4)
    per_device = local_experts * n_ep * most
    product = jnp.einsum(
        "tlnmf,lfd->tlnmd", by_source, down_weight, preferred_element_type=jnp.float32
    )
    own_sums = lax.psum_scatter(
        product.astype(jnp.bfloat16)
        .astype(jnp.float32)
        .reshape(per_device * lax.axis_size("tp"), width)
        .astype(jnp.bfloat16),
        "tp",
        scatter_dimension=0,
        tiled=True,
    )
    own_pieces = own_sums.reshape(local_experts, n_ep, most, width)
    back = lax.all_to_all(own_pieces, "ep", split_axis=1, concat_axis=0, tiled=True)
    picked = back.reshape(experts * most, width)[own_index].reshape(tok_rows, TOP_K, width)
    own_weights = lax.dynamic_slice_in_dim(route_weight, mine * tok_rows, tok_rows, 0)
    return weigh_pieces(picked.astype(jnp.float32), own_weights)


def neighbour(n, place, edge, piece):
    row, at, number = piece
    if edge == ACROSS:
        return place, (1 - row, at, number), ACROSS
    if edge == OUTWARD:
        return (place - 1, piece, INWARD) if place else None
    if place + 1 < n // 2:
        return place + 1, piece, OUTWARD
    return place, (row, n - 1 - at, number), INWARD


def parent(n, place, piece):
    row, at, number = piece
    if at == place:
        return ACROSS if row else None
    if row and CROSSES[min(at, n - 1 - at)][number]:
        return ACROSS
    return INWARD if at > place else OUTWARD


def children(n, place, piece):
    found = []
    for edge in (ACROSS, INWARD, OUTWARD):
        there = neighbour(n, place, edge, piece)
        if there is not None and parent(n, there[0], there[1]) == there[2]:
            found.append(edge)
    return found


def choose(index, low, branches):
    if len(branches) == 1:
        branches[0]()
        return
    half = len(branches) // 2
    pl.when(index < low + half)(lambda: choose(index, low, branches[:half]))
    pl.when(index >= low + half)(lambda: choose(index, low + half, branches[half:]))


def pick(index, values):
    result = values[0]
    for i, value in enumerate(values[1:], 1):
        result = jnp.where(index == i, value, result)
    return result


def split(order):
    before, steps, current = [], [], []
    for op in order:
        if op[0] == COMPUTE:
            before.append(current)
            steps.append(op[1:4])
            current = []
        else:
            current.append(op)
    return before, steps, current


def kernel(
    n, tok_hbm, gain_hbm, ids_hbm, weight_hbm, gate_hbm, up_hbm, down_hbm, out_ref,
    tok, gain, ids, weight, both, down, buf, own_shares, shares, part, srecv, rrecv,
    load_sem, w_s, w_r, ag_s, ag_r, ags_s, ags_r, rss_s, rss_r, rs_s, rs_r,
):
    ep = lax.axis_index("ep")
    z = lax.axis_index("tp")
    y, c = ep // 2, ep % 2
    rows, width = tok.shape
    inner = down.shape[0]
    experts = shares.shape[0]
    per = PIECES // UNITS
    tall = rows // UNITS
    short = rows // PIECES
    high = z // (n // 2)
    turn = 1 - 2 * high
    place = z + high * (n - 1 - 2 * z)
    sib = {"ep": 2 * y + 1 - c}
    toward = {ACROSS: {"ep": 2 * (1 - y) + c}, INWARD: {"tp": z + turn}, OUTWARD: {"tp": z - turn}}
    side = {ACROSS: 0, INWARD: 1 + high, OUTWARD: 2 - high}
    far_side = {ACROSS: 0, INWARD: 2 - high, OUTWARD: 1 + high}

    def block(row, at):
        return row + (1 - 2 * row) * y, at + high * (n - 1 - 2 * at)

    def remote(src, dst, send, recv, to):
        return pltpu.make_async_remote_copy(
            src_ref=src, dst_ref=dst, send_sem=send, recv_sem=recv, device_id=to, device_id_type=MESH
        )

    loads = [
        pltpu.make_async_copy(src, dst, load_sem.at[i])
        for i, (src, dst) in enumerate(
            (
                (tok_hbm, tok),
                (gain_hbm, gain),
                (ids_hbm, ids),
                (weight_hbm, weight),
                (gate_hbm.at[0], both.at[:, pl.ds(0, inner)]),
                (up_hbm.at[0], both.at[:, pl.ds(inner, inner)]),
                (down_hbm.at[0], down),
            )
        )
    ]
    for load in loads:
        load.start()

    barrier = pltpu.get_barrier_semaphore()
    for k in range(1, 4):
        pl.semaphore_signal(barrier, inc=1, device_id={"ep": (ep + k) % 4}, device_id_type=MESH)
    pl.semaphore_signal(barrier, inc=1, device_id=toward[INWARD], device_id_type=MESH)

    @pl.when(place > 0)
    def _():
        pl.semaphore_signal(barrier, inc=1, device_id=toward[OUTWARD], device_id_type=MESH)

    loads[0].wait()
    loads[1].wait()
    normed = norm_rows(tok[...], gain[...]).reshape(UNITS, per, short, width)
    for unit in range(UNITS):
        buf[y, z, unit, c] = normed[unit]
    loads[2].wait()
    loads[3].wait()
    for e in range(experts):
        named = jnp.where(ids[...] == e, weight[...], 0.0)
        total = named[0:1] + named[1:2]
        for k in range(n):
            own_shares[e, k : k + 1, :] = total[:, k * rows : (k + 1) * rows]

    pl.semaphore_wait(barrier, 4 + jnp.where(place > 0, 1, 0))

    def share(k):
        to = (ep + k) % 4
        return remote(own_shares.at[to], shares.at[ep], w_s.at[k], w_r.at[4 - k], {"ep": to})

    def copy_of(op):
        what, row, at, number, edge = op
        yb, zb = block(row, at)
        unit, piece = number // per, number % per
        if what == SEND:
            here = buf.at[yb, zb, unit, c, piece]
            return remote(here, here, ag_s.at[edge, yb, zb, number], ag_r.at[yb, zb, number], toward[edge])
        if what == RELAY:
            here = buf.at[yb, zb, unit, c, piece]
            return remote(here, here, ags_s.at[yb, zb, number], ags_r.at[yb, zb, number], sib)
        here = part.at[yb, zb, unit, c, piece]
        there = rrecv.at[far_side[edge], yb, zb, number]
        return remote(here, there, rs_s.at[yb, zb, number], rs_r.at[far_side[edge], yb, zb, number], toward[edge])

    def sum_copy(yb, zb, unit):
        return remote(part.at[yb, zb, unit, 1 - c], srecv.at[yb, zb, unit], rss_s.at[yb, zb, unit], rss_r.at[yb, zb, unit], sib)

    def run(here, ops, seen):
        for op in ops:
            what, row, at, number, edge = op
            yb, zb = block(row, at)
            unit, piece = number // per, number % per
            own = row == 0 and at == here
            if what == RELAY:
                if not own:
                    landed = buf.at[yb, zb, unit, c, piece]
                    remote(landed, landed, ags_s.at[yb, zb, number], ag_r.at[yb, zb, number], sib).wait_recv()
                copy_of(op).start()
            elif what == SEND:
                copy_of(op).start()
            else:
                if (row, at, unit) not in seen:
                    seen.add((row, at, unit))
                    sum_copy(yb, zb, unit).wait_recv()
                total = part[yb, zb, unit, c, piece].astype(jnp.float32)
                total = total + srecv[yb, zb, unit, piece].astype(jnp.float32)
                for child in children(n, here, (row, at, number)):
                    landed = rrecv.at[side[child], yb, zb, number]
                    remote(landed, landed, rs_s.at[yb, zb, number], rs_r.at[side[child], yb, zb, number], sib).wait_recv()
                    total = total + rrecv[side[child], yb, zb, number].astype(jnp.float32)
                if own:
                    out_ref[number * short : (number + 1) * short, :] = total.astype(out_ref.dtype)
                else:
                    part[yb, zb, unit, c, piece] = total.astype(jnp.bfloat16)
                    copy_of(op).start()

    plans = [split(order) for order in ORDER]
    steps = len(plans[0][1])
    branches, seen = [], [set() for _ in plans]
    for here, (before, _, _) in enumerate(plans):
        for ops in before:
            first = set()
            for op in ops:
                unit = (op[1], op[2], op[3] // per)
                if op[0] == REDUCE and unit not in seen[here]:
                    seen[here].add(unit)
                    first.add(unit)
            waited = {(r, a, u) for r in range(2) for a in range(n) for u in range(UNITS)} - first
            branches.append(functools.partial(run, here, ops, waited))

    def column(row):
        return jnp.transpose(jnp.broadcast_to(row, (rows, rows)))[:, :1]

    lane = lax.broadcasted_iota(jnp.int32, (8, rows), 1)

    def one(step, carry):
        choose(place * steps + step, 0, branches)

        @pl.when(step == 0)
        def _():
            for k in range(1, 4):
                share(k).start()
            shares[ep] = own_shares[ep]
            for k in range(1, 4):
                remote(own_shares.at[0], shares.at[(ep + k) % 4], w_s.at[k], w_r.at[k], sib).wait_recv()
            for load in loads[4:]:
                load.wait()

        row, at, unit = (
            pick(place, [pick(step, [s[i] for s in plan[1]]) for plan in plans]) for i in range(3)
        )
        yb, zb = block(row, at)
        for piece in range(per):
            landed = buf.at[yb, zb, unit, 1 - c, piece]
            number = unit * per + piece
            remote(landed, landed, ags_s.at[yb, zb, number], ags_r.at[yb, zb, number], sib).wait_recv()
        x = buf[yb, zb, unit].reshape(2 * tall, width)
        mixed = jnp.dot(x, both[...], preferred_element_type=jnp.float32)
        hidden = (jax.nn.silu(mixed[:, :inner]) * mixed[:, inner:]).astype(jnp.bfloat16)
        product = jnp.dot(hidden, down[...], preferred_element_type=jnp.float32)
        ours = [jnp.broadcast_to(shares[2 * yb + half, pl.ds(zb, 1), :], (8, rows)) for half in range(2)]
        turned = [pltpu.roll(values, tall, 1) for values in ours]
        first = jnp.where(lane < tall, ours[0], turned[1])
        second = jnp.where(lane < tall, turned[0], ours[1])
        w = column(jnp.where(unit == 0, first, second)[0:1])
        part[yb, zb, unit] = (product * w).astype(jnp.bfloat16).reshape(2, per, short, width)
        sum_copy(yb, zb, unit).start()
        return carry

    lax.fori_loop(0, steps, one, 0)

    def finish(here):
        after = plans[here][2]
        run(here, after, seen[here])
        for op in ORDER[here]:
            if op[0] in (RELAY, SEND) or (op[0] == REDUCE and parent(n, here, op[1:4]) is not None):
                copy_of(op).wait_send()

    choose(place, 0, [functools.partial(finish, here) for here in range(len(plans))])
    for k in range(1, 4):
        share(k).wait_send()
    for yb in range(2):
        for zb in range(n):
            for unit in range(UNITS):
                sum_copy(yb, zb, unit).wait_send()


def kernel_bytes(n, rows, width, inner):
    blocks = n * 4 + 2 * n * 2 + 2 * n + 6 * n + 4
    return 2 * width * (3 * inner + blocks * rows) + 16 * rows * (width + 2 * inner)


def fused_body(tokens, norm_gain, gate_weight, up_weight, down_weight, expert_ids, route_weight):
    rows, width = tokens.shape
    inner = gate_weight.shape[2]
    n = lax.axis_size("tp")
    experts = lax.axis_size("ep")
    vmem = pl.BlockSpec(memory_space=pltpu.VMEM)
    anywhere = pl.BlockSpec(memory_space=pl.ANY)
    dma = pltpu.SemaphoreType.DMA
    bf16 = jnp.bfloat16
    per, short = PIECES // UNITS, rows // PIECES
    return pl.pallas_call(
        functools.partial(kernel, n),
        out_shape=jax.ShapeDtypeStruct((rows, width), bf16),
        in_specs=[anywhere] * 7,
        out_specs=vmem,
        scratch_shapes=[
            pltpu.VMEM((rows, width), bf16),
            pltpu.VMEM((1, width), jnp.float32),
            pltpu.VMEM((TOP_K, n * rows), jnp.int32),
            pltpu.VMEM((TOP_K, n * rows), jnp.float32),
            pltpu.VMEM((width, 2 * inner), bf16),
            pltpu.VMEM((inner, width), bf16),
            pltpu.VMEM((2, n, UNITS, 2, per, short, width), bf16),
            pltpu.VMEM((experts, n, rows), jnp.float32),
            pltpu.VMEM((experts, n, rows), jnp.float32),
            pltpu.VMEM((2, n, UNITS, 2, per, short, width), bf16),
            pltpu.VMEM((2, n, UNITS, per, short, width), bf16),
            pltpu.VMEM((3, 2, n, PIECES, short, width), bf16),
            dma((7,)),
            dma((4,)),
            dma((4,)),
            dma((3, 2, n, PIECES)),
            dma((2, n, PIECES)),
            dma((2, n, PIECES)),
            dma((2, n, PIECES)),
            dma((2, n, UNITS)),
            dma((2, n, UNITS)),
            dma((2, n, PIECES)),
            dma((3, 2, n, PIECES)),
        ],
        compiler_params=pltpu.CompilerParams(
            collective_id=0, has_side_effects=True, vmem_limit_bytes=VMEM_ROOM
        ),
    )(tokens, norm_gain.reshape(1, width), expert_ids.T, route_weight.T, gate_weight, up_weight, down_weight)


def body(tokens, norm_gain, gate_weight, up_weight, down_weight, expert_ids, route_weight):
    rows, width = tokens.shape
    inner = gate_weight.shape[2]
    n = lax.axis_size("tp")
    fits = kernel_bytes(n, rows, width, inner) <= VMEM_ROOM and rows % 128 == 0
    chosen = plain_body
    if lax.axis_size("ep") == 4 and gate_weight.shape[0] == 1 and n == LINE and fits:
        chosen = fused_body
    return chosen(tokens, norm_gain, gate_weight, up_weight, down_weight, expert_ids, route_weight)


def solution(mesh):
    placed = (
        P(("grp", "ep", "tp"), None),
        P(),
        P("ep", None, "tp"),
        P("ep", None, "tp"),
        P("ep", "tp", None),
        P(("grp", "ep"), None),
        P(("grp", "ep"), None),
    )
    return jax.shard_map(
        body, mesh=mesh, in_specs=placed, out_specs=P(("grp", "ep", "tp"), None), check_vma=False
    )
```

time: 76.4 us -> 56.2 us (0.74)
  the two profiles are of different devices: /device:TPU:25 before, /device:TPU:0 now
where the time goes in v1:
time: 56.2 us; the launch traced here: 56 us
  Pallas kernels  54.4 us (97%)
  local copies, waits for them, and re-layouts  1.67 us (3%)
    pallas_call x1, Pallas kernels, fused_body(): pl.pallas_call(functools.partial(kernel, n), out_shape=jax.ShapeDtypeStru...  54.4 us
    unnamed x1, local copies, waits for them, and re-layouts  1.67 us

profile of v1, /device:TPU:0, one launch (start us, length us, event | category | flops | bytes accessed | tf_op | source)
XLA Modules:
  0.0 56.0 jit_solution(5821910278649706839)
XLA Ops:
  0.0 54.4 %shard_map.73 = bf16[128,1024]{1,0:T(8,128)(2,1)} custom-call(bf16[128,1024]{1,0:T(8,128)(2,1)} %tok_hbm.1, f32[1,1024]{1,0:T(1,128)} %bitcast.3, s32[2,512]{1,0:T(2,128)} %bitcast.4, f32[2,512]{1,0:T(2,128)} %bitcast.5, bf16[1,1024,896]{2,1,0:T(8,128)(2,1)} %gate_hbm.1, bf16[1,1024,896]{2,1,0:T(8,128)(2,1)} %up_hbm.1, bf16[1,896,1024]{2,1,0:T(8,128)(2,1)} %down_hbm.1), custom_call_target="tpu_custom_call" | custom-call | tf_op jit(solution)/shard_map/pallas_call | solution.py:401
  54.4 1.7 %copy.9 = bf16[128,1024]{1,0:T(8,128)(2,1)} copy(bf16[128,1024]{1,0:T(8,128)(2,1)} %shard_map.73) | data formatting | bytes 524288

commit v2 on v1

v2 whole, which is shorter than its diff:
```python
import functools

import jax
import jax.numpy as jnp
from jax import lax
from jax.experimental import pallas as pl
from jax.experimental.pallas import tpu as pltpu
from jax.sharding import PartitionSpec as P

TOP_K = 2
MESH = pl.DeviceIdType.MESH
VMEM_ROOM = 60 << 20

ACROSS, UP, DOWN = range(3)
RELAY, SEND, REDUCE, COMPUTE = range(4)
UNITS = 2
PIECES = 4
LINE = 4
SPREAD = ((11, 5, 14, 7), (11, 1, 7, 13), (15, 3, 8, 14), (11, 8, 13, 11))
GATHER = ((8, 11, 15, 1), (12, 14, 12, 11), (15, 12, 3, 3), (12, 5, 7, 1))
ORDER = (
    (
        (0, 0, 0, 0, 0), (0, 0, 0, 1, 0), (0, 0, 0, 2, 0), (0, 0, 0, 3, 0), (1, 0, 0, 0, 1), (1, 0, 0, 3, 0),
        (1, 0, 0, 1, 1), (1, 0, 0, 0, 0), (3, 0, 0, 0, 0), (1, 0, 0, 3, 1), (1, 0, 0, 1, 0), (3, 0, 0, 1, 0),
        (1, 0, 0, 2, 1), (0, 1, 0, 3, 0), (0, 0, 1, 3, 0), (1, 0, 1, 3, 0), (0, 1, 0, 0, 0), (0, 0, 1, 2, 0),
        (1, 0, 1, 2, 0), (0, 1, 0, 1, 0), (1, 1, 0, 1, 1), (3, 0, 1, 1, 0), (0, 0, 1, 1, 0), (0, 1, 1, 3, 0),
        (1, 0, 1, 1, 0), (1, 1, 1, 3, 1), (3, 1, 0, 0, 0), (2, 0, 1, 2, 1), (0, 0, 2, 2, 0), (0, 1, 1, 2, 0),
        (0, 0, 1, 0, 0), (1, 0, 1, 0, 0), (2, 1, 0, 0, 1), (2, 1, 0, 1, 0), (3, 1, 1, 1, 0), (0, 1, 1, 1, 0),
        (0, 0, 2, 0, 0), (1, 1, 1, 1, 1), (1, 0, 2, 0, 0), (3, 0, 1, 0, 0), (2, 1, 1, 2, 1), (2, 1, 1, 3, 0),
        (0, 0, 2, 1, 0), (0, 1, 1, 0, 0), (2, 0, 1, 1, 1), (0, 0, 3, 0, 0), (3, 0, 2, 0, 0), (2, 0, 1, 0, 1),
        (1, 0, 3, 0, 0), (3, 1, 1, 0, 0), (0, 0, 3, 2, 0), (0, 1, 2, 0, 0), (2, 0, 2, 1, 1), (1, 0, 2, 1, 0),
        (0, 0, 3, 3, 0), (1, 0, 3, 3, 0), (2, 1, 1, 1, 1), (3, 0, 3, 1, 0), (0, 1, 0, 2, 0), (0, 1, 3, 0, 0),
        (1, 0, 3, 2, 0), (2, 0, 1, 3, 1), (0, 1, 3, 1, 0), (0, 1, 2, 1, 0), (3, 1, 0, 1, 0), (0, 0, 3, 1, 0),
        (2, 1, 1, 0, 1), (3, 1, 3, 0, 0), (2, 1, 0, 2, 0), (0, 0, 2, 3, 0), (0, 1, 3, 3, 0), (3, 1, 2, 0, 0),
        (2, 1, 3, 0, 1), (2, 1, 3, 1, 0), (0, 1, 2, 2, 0), (0, 1, 3, 2, 0), (3, 0, 3, 0, 0), (2, 1, 2, 0, 0),
        (2, 1, 2, 1, 1), (0, 1, 2, 3, 0), (3, 1, 3, 1, 0), (2, 0, 3, 0, 1), (3, 0, 2, 1, 0), (2, 0, 3, 1, 1),
        (2, 1, 3, 2, 0), (3, 1, 2, 1, 0), (2, 0, 2, 0, 1), (2, 1, 3, 3, 0), (2, 1, 2, 3, 0), (2, 1, 2, 2, 0),
        (2, 0, 3, 2, 1), (2, 0, 3, 3, 1), (2, 0, 2, 3, 1), (2, 1, 0, 3, 0), (2, 0, 2, 2, 1), (2, 0, 0, 1, 0),
        (2, 0, 0, 3, 0), (2, 0, 0, 2, 0), (2, 0, 0, 0, 0),
    ),
    (
        (0, 0, 1, 1, 0), (0, 0, 1, 0, 0), (0, 0, 1, 2, 0), (0, 0, 1, 3, 0), (1, 0, 1, 3, 1), (1, 0, 1, 3, 2),
        (1, 0, 1, 0, 0), (1, 0, 1, 2, 1), (1, 0, 1, 2, 2), (1, 0, 1, 2, 0), (3, 0, 1, 0, 0), (1, 0, 1, 1, 2),
        (1, 0, 1, 0, 1), (3, 0, 1, 1, 0), (0, 0, 0, 0, 0), (0, 0, 2, 2, 0), (1, 0, 0, 0, 0), (0, 1, 1, 0, 0),
        (1, 0, 2, 2, 2), (1, 0, 0, 0, 1), (0, 0, 0, 1, 0), (1, 0, 0, 1, 1), (1, 0, 1, 0, 2), (0, 0, 2, 0, 0),
        (1, 0, 2, 0, 0), (0, 1, 1, 2, 0), (3, 0, 0, 0, 0), (0, 0, 0, 3, 0), (1, 0, 0, 3, 0), (1, 0, 0, 3, 1),
        (1, 0, 2, 0, 2), (0, 0, 2, 1, 0), (1, 0, 2, 1, 0), (0, 0, 0, 2, 0), (0, 1, 0, 0, 0), (1, 0, 0, 2, 1),
        (1, 0, 2, 1, 2), (3, 0, 2, 0, 0), (0, 0, 3, 0, 0), (0, 1, 2, 0, 0), (0, 1, 0, 1, 0), (1, 0, 0, 2, 0),
        (3, 0, 0, 1, 0), (0, 0, 2, 3, 0), (0, 1, 0, 3, 0), (1, 0, 3, 0, 2), (1, 0, 3, 0, 0), (1, 1, 0, 0, 1),
        (3, 1, 0, 0, 0), (0, 0, 3, 2, 0), (0, 1, 2, 1, 0), (0, 1, 1, 3, 0), (1, 0, 3, 2, 2), (1, 0, 2, 3, 0),
        (1, 1, 2, 1, 1), (3, 0, 2, 1, 0), (0, 0, 3, 3, 0), (0, 1, 0, 2, 0), (1, 0, 3, 3, 2), (3, 1, 2, 0, 0),
        (2, 1, 0, 0, 1), (0, 0, 3, 1, 0), (0, 1, 3, 0, 0), (1, 1, 0, 2, 2), (1, 0, 1, 1, 1), (3, 0, 3, 1, 0),
        (2, 1, 2, 0, 0), (0, 1, 1, 1, 0), (0, 1, 2, 3, 0), (0, 1, 3, 1, 0), (1, 1, 3, 1, 2), (1, 1, 1, 1, 1),
        (1, 0, 3, 3, 0), (3, 1, 0, 1, 0), (0, 1, 3, 2, 0), (1, 0, 3, 1, 2), (3, 1, 3, 0, 0), (1, 0, 2, 3, 2),
        (1, 1, 1, 0, 1), (2, 1, 0, 2, 0), (0, 1, 2, 2, 0), (3, 0, 3, 0, 0), (2, 1, 3, 1, 1), (1, 1, 2, 2, 2),
        (3, 1, 1, 0, 0), (0, 1, 3, 3, 0), (1, 1, 2, 3, 2), (3, 1, 1, 1, 0), (2, 0, 2, 1, 1), (3, 1, 3, 1, 0),
        (2, 1, 1, 1, 0), (2, 1, 1, 2, 1), (2, 1, 1, 3, 0), (3, 1, 2, 1, 0), (2, 1, 3, 2, 0), (2, 1, 3, 3, 2),
        (2, 1, 1, 0, 1), (2, 1, 0, 1, 0), (2, 1, 3, 0, 1), (2, 1, 2, 3, 0), (2, 1, 2, 1, 1), (2, 1, 2, 2, 0),
        (2, 0, 0, 3, 2), (2, 0, 3, 0, 1), (2, 1, 0, 3, 2), (2, 0, 3, 1, 1), (2, 0, 2, 0, 1), (2, 0, 0, 1, 2),
        (2, 0, 3, 2, 1), (2, 0, 0, 2, 2), (2, 0, 3, 3, 1), (2, 0, 0, 0, 2), (2, 0, 2, 3, 1), (2, 0, 1, 2, 0),
        (2, 0, 2, 2, 1), (2, 0, 1, 3, 0), (2, 0, 1, 1, 0), (2, 0, 1, 0, 0),
    ),
    (
        (1, 0, 2, 2, 2), (0, 0, 2, 2, 0), (0, 0, 2, 1, 0), (0, 0, 2, 0, 0), (0, 0, 2, 3, 0), (1, 0, 2, 2, 1),
        (1, 0, 2, 3, 0), (1, 0, 2, 0, 2), (1, 0, 2, 1, 1), (1, 0, 2, 0, 0), (3, 0, 2, 0, 0), (1, 0, 2, 0, 1),
        (1, 0, 2, 1, 2), (3, 0, 2, 1, 0), (0, 0, 3, 0, 0), (0, 0, 1, 3, 0), (0, 1, 2, 3, 0), (1, 0, 1, 3, 0),
        (1, 0, 3, 0, 2), (1, 0, 1, 3, 1), (1, 0, 2, 3, 2), (1, 0, 2, 3, 1), (0, 0, 1, 2, 0), (1, 0, 1, 2, 0),
        (0, 0, 3, 2, 0), (0, 1, 2, 0, 0), (1, 0, 3, 2, 0), (1, 0, 3, 2, 2), (3, 0, 1, 1, 0), (0, 0, 3, 3, 0),
        (0, 0, 1, 0, 0), (0, 1, 1, 3, 0), (1, 0, 1, 2, 1), (1, 0, 3, 3, 2), (1, 0, 1, 0, 1), (0, 0, 0, 0, 0),
        (0, 0, 3, 1, 0), (3, 0, 3, 1, 0), (0, 0, 0, 1, 0), (0, 1, 1, 2, 0), (0, 1, 3, 3, 0), (1, 0, 0, 0, 1),
        (1, 0, 0, 1, 0), (1, 0, 3, 1, 2), (3, 0, 3, 0, 0), (0, 0, 0, 3, 0), (0, 1, 3, 2, 0), (0, 1, 3, 1, 0),
        (1, 0, 0, 3, 0), (1, 1, 3, 1, 2), (1, 0, 0, 3, 1), (3, 0, 0, 0, 0), (0, 0, 0, 2, 0), (1, 0, 0, 2, 1),
        (1, 1, 3, 2, 2), (0, 1, 3, 0, 0), (1, 0, 0, 2, 0), (3, 1, 3, 1, 0), (0, 1, 0, 1, 0), (0, 1, 0, 0, 0),
        (1, 1, 0, 1, 1), (3, 0, 0, 1, 0), (0, 1, 2, 2, 0), (0, 1, 0, 3, 0), (1, 1, 2, 2, 2), (3, 1, 3, 0, 0),
        (0, 1, 2, 1, 0), (0, 1, 0, 2, 0), (1, 1, 0, 3, 1), (3, 1, 1, 1, 0), (2, 1, 3, 2, 0), (1, 0, 0, 1, 1),
        (3, 1, 0, 0, 0), (2, 1, 1, 3, 2), (1, 1, 1, 2, 1), (3, 1, 0, 1, 0), (2, 1, 0, 1, 2), (2, 1, 0, 0, 1),
        (0, 0, 1, 1, 0), (3, 1, 2, 1, 0), (2, 1, 0, 2, 0), (2, 1, 3, 3, 2), (0, 1, 1, 1, 0), (1, 1, 1, 1, 1),
        (3, 0, 1, 0, 0), (2, 1, 2, 3, 2), (0, 1, 1, 0, 0), (1, 0, 1, 1, 1), (3, 1, 2, 0, 0), (2, 1, 2, 2, 2),
        (2, 1, 3, 1, 0), (1, 1, 2, 1, 1), (3, 1, 1, 0, 0), (2, 1, 2, 0, 0), (2, 0, 0, 3, 2), (2, 1, 1, 2, 0),
        (2, 1, 1, 1, 0), (2, 1, 0, 3, 2), (2, 1, 1, 0, 0), (2, 0, 0, 1, 2), (2, 1, 3, 0, 0), (2, 0, 0, 2, 2),
        (2, 1, 2, 1, 0), (2, 0, 0, 0, 2), (2, 0, 1, 2, 2), (2, 0, 3, 0, 1), (2, 0, 3, 1, 1), (2, 0, 1, 3, 2),
        (2, 0, 1, 1, 2), (2, 0, 3, 2, 1), (2, 0, 1, 0, 2), (2, 0, 3, 3, 1), (2, 0, 2, 1, 0), (2, 0, 2, 3, 0),
        (2, 0, 2, 0, 0), (2, 0, 2, 2, 0),
    ),
    (
        (0, 0, 3, 0, 0), (0, 0, 3, 1, 0), (0, 0, 3, 2, 0), (0, 0, 3, 3, 0), (1, 0, 3, 0, 2), (1, 0, 3, 3, 0),
        (1, 0, 3, 2, 2), (1, 0, 3, 1, 0), (3, 0, 3, 0, 0), (1, 0, 3, 3, 2), (1, 0, 3, 0, 0), (3, 0, 3, 1, 0),
        (1, 0, 3, 1, 2), (1, 0, 3, 2, 0), (0, 0, 2, 2, 0), (0, 1, 3, 3, 0), (1, 1, 3, 3, 2), (1, 0, 2, 2, 0),
        (0, 1, 3, 1, 0), (0, 0, 2, 1, 0), (1, 1, 3, 1, 2), (0, 0, 2, 0, 0), (0, 1, 3, 0, 0), (1, 0, 2, 0, 0),
        (1, 1, 3, 0, 2), (3, 0, 2, 0, 0), (0, 0, 1, 3, 0), (0, 1, 3, 2, 0), (1, 0, 1, 3, 0), (3, 1, 3, 0, 0),
        (0, 1, 2, 2, 0), (0, 0, 2, 3, 0), (1, 0, 2, 3, 0), (1, 1, 2, 2, 2), (3, 1, 3, 1, 0), (2, 1, 3, 0, 0),
        (2, 1, 3, 1, 2), (0, 0, 1, 2, 0), (0, 1, 2, 0, 0), (3, 0, 2, 1, 0), (2, 1, 3, 2, 2), (0, 0, 1, 0, 0),
        (0, 1, 1, 3, 0), (1, 0, 1, 0, 0), (3, 0, 1, 1, 0), (2, 0, 2, 3, 2), (0, 0, 0, 0, 0), (0, 1, 2, 3, 0),
        (1, 0, 0, 0, 0), (2, 0, 2, 2, 2), (0, 0, 0, 3, 0), (3, 1, 2, 1, 0), (2, 1, 3, 3, 2), (0, 0, 0, 2, 0),
        (1, 0, 0, 2, 0), (0, 1, 1, 0, 0), (2, 1, 2, 3, 2), (3, 0, 0, 1, 0), (0, 1, 0, 0, 0), (0, 1, 0, 1, 0),
        (2, 1, 2, 2, 2), (0, 1, 0, 3, 0), (0, 1, 0, 2, 0), (3, 1, 0, 0, 0), (2, 0, 0, 3, 2), (0, 0, 0, 1, 0),
        (3, 1, 0, 1, 0), (2, 1, 0, 1, 0), (0, 1, 1, 2, 0), (3, 0, 0, 0, 0), (2, 1, 0, 2, 0), (2, 1, 0, 3, 2),
        (3, 1, 1, 1, 0), (2, 1, 0, 0, 0), (0, 1, 1, 1, 0), (2, 0, 0, 1, 2), (2, 1, 1, 2, 0), (3, 1, 1, 0, 0),
        (2, 1, 1, 3, 0), (2, 0, 0, 2, 2), (0, 0, 1, 1, 0), (0, 1, 2, 1, 0), (2, 1, 1, 1, 0), (2, 0, 0, 0, 2),
        (3, 0, 1, 0, 0), (2, 1, 1, 0, 0), (2, 0, 1, 2, 2), (3, 1, 2, 0, 0), (2, 0, 1, 3, 2), (2, 1, 2, 1, 0),
        (2, 1, 2, 0, 0), (2, 0, 1, 1, 2), (2, 0, 1, 0, 2), (2, 0, 2, 1, 2), (2, 0, 2, 0, 2), (2, 0, 3, 0, 0),
        (2, 0, 3, 1, 0), (2, 0, 3, 2, 0), (2, 0, 3, 3, 0),
    ),
)


def norm_rows(tokens, norm_gain):
    values = tokens.astype(jnp.float32)
    scaled = values * lax.rsqrt(jnp.mean(values * values, axis=-1, keepdims=True) + 1e-06)
    return (scaled * norm_gain).astype(jnp.bfloat16)


def expert_hidden(rows, gate_weight, up_weight):
    gate = jnp.einsum("e...d,edf->e...f", rows, gate_weight, preferred_element_type=jnp.float32)
    upper = jnp.einsum("e...d,edf->e...f", rows, up_weight, preferred_element_type=jnp.float32)
    return (jax.nn.silu(gate) * upper).astype(jnp.bfloat16)


def weigh_pieces(summed, weights):
    piece = lax.optimization_barrier(summed.astype(jnp.bfloat16)).astype(jnp.float32)
    total = piece[:, 0] * weights[:, 0:1]
    total = total + piece[:, 1] * weights[:, 1:2]
    return total.astype(jnp.bfloat16)


def plain_body(tokens, norm_gain, gate_weight, up_weight, down_weight, expert_ids, route_weight):
    tok_rows = tokens.shape[0]
    width = tokens.shape[1]
    local_experts = gate_weight.shape[0]
    inner = gate_weight.shape[2]
    n_tp = lax.axis_size("tp")
    n_ep = lax.axis_size("ep")
    experts = n_ep * local_experts
    most = max(2, tok_rows * TOP_K * 5 // (4 * experts))
    normed = norm_rows(tokens, norm_gain)
    flat_ids = expert_ids.reshape(n_tp, tok_rows * TOP_K)
    onehot = (flat_ids[:, :, None] == jnp.arange(experts, dtype=jnp.int32)[None, None, :]).astype(
        jnp.int32
    )
    before = jnp.cumsum(onehot, axis=1) - onehot
    slots = jnp.sum(before * onehot, axis=-1)
    owner = jnp.arange(n_tp, dtype=jnp.int32)[:, None]
    row_index = (flat_ids * (n_tp * most) + owner * most + slots).reshape(-1)
    mine = lax.axis_index("tp")
    own_ids = lax.dynamic_slice_in_dim(flat_ids, mine, 1, 0)[0]
    own_slots = lax.dynamic_slice_in_dim(slots, mine, 1, 0)[0]
    own_index = own_ids * most + own_slots
    whole = lax.all_gather(normed, "tp", axis=0, tiled=True)
    sending = (
        jnp.zeros((experts * n_tp * most, width), jnp.bfloat16)
        .at[row_index]
        .set(jnp.repeat(whole, TOP_K, axis=0))
    )
    arrived = lax.all_to_all(
        sending.reshape(experts, n_tp * most, width), "ep", split_axis=0, concat_axis=1, tiled=True
    )
    hidden = expert_hidden(arrived, gate_weight, up_weight)
    by_source = hidden.reshape(local_experts, n_ep, n_tp, most, inner).transpose(2, 0, 1, 3, 4)
    per_device = local_experts * n_ep * most
    product = jnp.einsum(
        "tlnmf,lfd->tlnmd", by_source, down_weight, preferred_element_type=jnp.float32
    )
    own_sums = lax.psum_scatter(
        product.astype(jnp.bfloat16)
        .astype(jnp.float32)
        .reshape(per_device * lax.axis_size("tp"), width)
        .astype(jnp.bfloat16),
        "tp",
        scatter_dimension=0,
        tiled=True,
    )
    own_pieces = own_sums.reshape(local_experts, n_ep, most, width)
    back = lax.all_to_all(own_pieces, "ep", split_axis=1, concat_axis=0, tiled=True)
    picked = back.reshape(experts * most, width)[own_index].reshape(tok_rows, TOP_K, width)
    own_weights = lax.dynamic_slice_in_dim(route_weight, mine * tok_rows, tok_rows, 0)
    return weigh_pieces(picked.astype(jnp.float32), own_weights)


def neighbour(n, place, edge, piece):
    row, at, number = piece
    if edge == ACROSS:
        return place, (1 - row, at, number), ACROSS
    there = place + (1 if edge == UP else -1)
    return (there, piece, DOWN if edge == UP else UP) if 0 <= there < n else None


def parent(n, crossings, place, piece):
    row, at, number = piece
    goal = at
    if row:
        bits = crossings[at][number]
        places = [k for k in range(n) if bits >> k & 1]
        goal = min(places, key=lambda k: (abs(k - place), abs(k - at)))
    if goal == place:
        return ACROSS if row else None
    return UP if goal > place else DOWN


def children(n, crossings, place, piece):
    found = []
    for edge in (ACROSS, UP, DOWN):
        there = neighbour(n, place, edge, piece)
        if there is not None and parent(n, crossings, there[0], there[1]) == there[2]:
            found.append(edge)
    return found


def choose(index, low, branches):
    if len(branches) == 1:
        branches[0]()
        return
    half = len(branches) // 2
    pl.when(index < low + half)(lambda: choose(index, low, branches[:half]))
    pl.when(index >= low + half)(lambda: choose(index, low + half, branches[half:]))


def pick(index, values):
    result = values[0]
    for i, value in enumerate(values[1:], 1):
        result = jnp.where(index == i, value, result)
    return result


def split(order):
    before, steps, current = [], [], []
    for op in order:
        if op[0] == COMPUTE:
            before.append(current)
            steps.append(op[1:4])
            current = []
        else:
            current.append(op)
    return before, steps, current


def kernel(
    n, tok_hbm, gain_hbm, ids_hbm, weight_hbm, gate_hbm, up_hbm, down_hbm, out_ref,
    tok, gain, ids, weight, both, down, buf, own_shares, shares, part, srecv, rrecv,
    load_sem, w_s, w_r, sib_s, ag_s, rs_s, ag_r, ags_r, rss_r, rs_r,
):
    ep = lax.axis_index("ep")
    z = lax.axis_index("tp")
    y, c = ep // 2, ep % 2
    rows, width = tok.shape
    inner = down.shape[0]
    experts = shares.shape[0]
    per = PIECES // UNITS
    tall = rows // UNITS
    short = rows // PIECES
    sib = {"ep": 2 * y + 1 - c}
    toward = {ACROSS: {"ep": 2 * (1 - y) + c}, UP: {"tp": z + 1}, DOWN: {"tp": z - 1}}

    def row_of(row):
        return row + (1 - 2 * row) * y

    def first(row, at, unit, lane):
        return (((row * n + at) * UNITS + unit) * 2 + lane) * per

    def remote(src, dst, send, recv, to):
        return pltpu.make_async_remote_copy(
            src_ref=src, dst_ref=dst, send_sem=send, recv_sem=recv, device_id=to, device_id_type=MESH
        )

    loads = [
        pltpu.make_async_copy(src, dst, load_sem.at[i])
        for i, (src, dst) in enumerate(
            (
                (tok_hbm, tok),
                (gain_hbm, gain),
                (ids_hbm, ids),
                (weight_hbm, weight),
                (gate_hbm.at[0], both.at[:, pl.ds(0, inner)]),
                (up_hbm.at[0], both.at[:, pl.ds(inner, inner)]),
                (down_hbm.at[0], down),
            )
        )
    ]
    for load in loads:
        load.start()

    barrier = pltpu.get_barrier_semaphore()
    for k in range(1, 4):
        pl.semaphore_signal(barrier, inc=1, device_id={"ep": (ep + k) % 4}, device_id_type=MESH)

    @pl.when(z < n - 1)
    def _():
        pl.semaphore_signal(barrier, inc=1, device_id=toward[UP], device_id_type=MESH)

    @pl.when(z > 0)
    def _():
        pl.semaphore_signal(barrier, inc=1, device_id=toward[DOWN], device_id_type=MESH)

    loads[0].wait()
    loads[1].wait()
    normed = norm_rows(tok[...], gain[...]).reshape(UNITS, per, short, width)
    for unit in range(UNITS):
        buf[pl.ds(first(y, z, unit, c), per)] = normed[unit]
    loads[2].wait()
    loads[3].wait()
    for e in range(experts):
        named = jnp.where(ids[...] == e, weight[...], 0.0)
        total = named[0:1] + named[1:2]
        for k in range(n):
            own_shares[e, k : k + 1, :] = total[:, k * rows : (k + 1) * rows]

    pl.semaphore_wait(barrier, 3 + jnp.where(z > 0, 1, 0) + jnp.where(z < n - 1, 1, 0))

    def share(k):
        to = (ep + k) % 4
        return remote(own_shares.at[to], shares.at[ep], w_s, w_r, {"ep": to})

    def held(yb, at, number, lane):
        return buf.at[first(yb, at, number // per, lane) + number % per]

    def sum_copy(yb, at, unit):
        return remote(part.at[yb, at, unit, 1 - c], srecv.at[yb, at, unit], sib_s, rss_r.at[yb, at, unit], sib)

    def run(here, ops, waited):
        waited = set(waited)
        for op in ops:
            what, row, at, number, edge = op
            yb = row_of(row)
            unit, piece = number // per, number % per
            mine = held(yb, at, number, c)
            own = row == 0 and at == here
            if what == RELAY:
                if not own:
                    remote(mine, mine, ag_s, ag_r.at[yb, at, number], sib).wait_recv()
                remote(mine, mine, sib_s, ags_r.at[yb, at, unit], sib).start()
            elif what == SEND:
                remote(mine, mine, ag_s, ag_r.at[yb, at, number], toward[edge]).start()
            else:
                if (row, at, unit) not in waited:
                    waited.add((row, at, unit))
                    sum_copy(yb, at, unit).wait_recv()
                total = part[yb, at, unit, c, piece].astype(jnp.float32)
                total = total + srecv[yb, at, unit, piece].astype(jnp.float32)
                count = len(children(n, GATHER, here, (row, at, number)))
                if count:
                    landed = rrecv.at[yb, at, number, pl.ds(0, count)]
                    remote(landed, landed, rs_s, rs_r.at[yb, at, number], sib).wait_recv()
                for slot in range(count):
                    total = total + rrecv[yb, at, number, slot].astype(jnp.float32)
                if own:
                    out_ref[number * short : (number + 1) * short, :] = total.astype(out_ref.dtype)
                else:
                    part[yb, at, unit, c, piece] = total.astype(jnp.bfloat16)
                    there, seen_as, back = neighbour(n, here, edge, (row, at, number))
                    slot = children(n, GATHER, there, seen_as).index(back)
                    remote(
                        part.at[yb, at, unit, c, piece], rrecv.at[yb, at, number, slot],
                        rs_s, rs_r.at[yb, at, number], toward[edge],
                    ).start()

    plans = [split(order) for order in ORDER]
    steps = len(plans[0][1])
    branches, waited = [], [set() for _ in plans]
    for here, (before, _, _) in enumerate(plans):
        for ops in before:
            branches.append(functools.partial(run, here, ops, waited[here]))
            waited[here] = waited[here] | {(op[1], op[2], op[3] // per) for op in ops if op[0] == REDUCE}

    def column(row):
        return jnp.transpose(jnp.broadcast_to(row, (rows, rows)))[:, :1]

    lane = lax.broadcasted_iota(jnp.int32, (8, rows), 1)

    def one(step, carry):
        choose(z * steps + step, 0, branches)

        @pl.when(step == 0)
        def _():
            for k in range(1, 4):
                share(k).start()
            shares[ep] = own_shares[ep]
            remote(own_shares.at[pl.ds(0, 3)], shares.at[pl.ds(0, 3)], w_s, w_r, sib).wait_recv()
            for load in loads[4:]:
                load.wait()

        row, at, unit = (
            pick(z, [pick(step, [s[i] for s in plan[1]]) for plan in plans]) for i in range(3)
        )
        yb = row_of(row)
        theirs = buf.at[pl.ds(first(yb, at, unit, 1 - c), per)]
        remote(theirs, theirs, sib_s, ags_r.at[yb, at, unit], sib).wait_recv()
        x = buf[pl.ds(first(yb, at, unit, 0), 2 * per)].reshape(2 * tall, width)
        mixed = jnp.dot(x, both[...], preferred_element_type=jnp.float32)
        hidden = (jax.nn.silu(mixed[:, :inner]) * mixed[:, inner:]).astype(jnp.bfloat16)
        product = jnp.dot(hidden, down[...], preferred_element_type=jnp.float32)
        ours = [jnp.broadcast_to(shares[2 * yb + half, pl.ds(at, 1), :], (8, rows)) for half in range(2)]
        turned = [pltpu.roll(values, tall, 1) for values in ours]
        early = jnp.where(lane < tall, ours[0], turned[1])
        late = jnp.where(lane < tall, turned[0], ours[1])
        w = column(jnp.where(unit == 0, early, late)[0:1])
        part[yb, at, unit] = (product * w).astype(jnp.bfloat16).reshape(2, per, short, width)
        sum_copy(yb, at, unit).start()
        return carry

    lax.fori_loop(0, steps, one, 0)

    def finish(here):
        run(here, plans[here][2], waited[here])
        for what, sem in ((SEND, ag_s), (REDUCE, rs_s)):
            count = sum(op[0] == what and (what == SEND or op[1] > 0 or op[2] != here) for op in ORDER[here])
            sent = buf.at[pl.ds(0, count)]
            remote(sent, sent, sem, sem, sib).wait_send()

    choose(z, 0, [functools.partial(finish, here) for here in range(len(plans))])
    remote(buf, buf, sib_s, sib_s, sib).wait_send()
    remote(own_shares.at[pl.ds(0, 3)], shares.at[pl.ds(0, 3)], w_s, w_r, sib).wait_send()


def kernel_bytes(n, rows, width, inner):
    blocks = n * 4 + 2 * n * 2 + 2 * n + 6 * n + 4
    return 2 * width * (3 * inner + blocks * rows) + 16 * rows * (width + 2 * inner)


def fused_body(tokens, norm_gain, gate_weight, up_weight, down_weight, expert_ids, route_weight):
    rows, width = tokens.shape
    inner = gate_weight.shape[2]
    n = lax.axis_size("tp")
    experts = lax.axis_size("ep")
    vmem = pl.BlockSpec(memory_space=pltpu.VMEM)
    anywhere = pl.BlockSpec(memory_space=pl.ANY)
    dma = pltpu.SemaphoreType.DMA
    bf16 = jnp.bfloat16
    per, short = PIECES // UNITS, rows // PIECES
    return pl.pallas_call(
        functools.partial(kernel, n),
        out_shape=jax.ShapeDtypeStruct((rows, width), bf16),
        in_specs=[anywhere] * 7,
        out_specs=vmem,
        scratch_shapes=[
            pltpu.VMEM((rows, width), bf16),
            pltpu.VMEM((1, width), jnp.float32),
            pltpu.VMEM((TOP_K, n * rows), jnp.int32),
            pltpu.VMEM((TOP_K, n * rows), jnp.float32),
            pltpu.VMEM((width, 2 * inner), bf16),
            pltpu.VMEM((inner, width), bf16),
            pltpu.VMEM((2 * n * UNITS * 2 * per, short, width), bf16),
            pltpu.VMEM((experts, n, rows), jnp.float32),
            pltpu.VMEM((experts, n, rows), jnp.float32),
            pltpu.VMEM((2, n, UNITS, 2, per, short, width), bf16),
            pltpu.VMEM((2, n, UNITS, per, short, width), bf16),
            pltpu.VMEM((2, n, PIECES, 3, short, width), bf16),
            dma((7,)),
            dma,
            dma,
            dma,
            dma,
            dma,
            dma((2, n, PIECES)),
            dma((2, n, UNITS)),
            dma((2, n, UNITS)),
            dma((2, n, PIECES)),
        ],
        compiler_params=pltpu.CompilerParams(
            collective_id=0, has_side_effects=True, vmem_limit_bytes=VMEM_ROOM
        ),
    )(tokens, norm_gain.reshape(1, width), expert_ids.T, route_weight.T, gate_weight, up_weight, down_weight)


def body(tokens, norm_gain, gate_weight, up_weight, down_weight, expert_ids, route_weight):
    rows, width = tokens.shape
    inner = gate_weight.shape[2]
    n = lax.axis_size("tp")
    fits = kernel_bytes(n, rows, width, inner) <= VMEM_ROOM and rows % 128 == 0
    chosen = plain_body
    if lax.axis_size("ep") == 4 and gate_weight.shape[0] == 1 and n == LINE and fits:
        chosen = fused_body
    return chosen(tokens, norm_gain, gate_weight, up_weight, down_weight, expert_ids, route_weight)


def solution(mesh):
    placed = (
        P(("grp", "ep", "tp"), None),
        P(),
        P("ep", None, "tp"),
        P("ep", None, "tp"),
        P("ep", "tp", None),
        P(("grp", "ep"), None),
        P(("grp", "ep"), None),
    )
    return jax.shard_map(
        body, mesh=mesh, in_specs=placed, out_specs=P(("grp", "ep", "tp"), None), check_vma=False
    )
```

time: 56.2 us -> 50.8 us (0.904)
  Pallas kernels: 54.4 us -> 49 us
    pallas_call x1, Pallas kernels: 54.4 us -> 49 us  [fused_body(): pl.pallas_call(functools.partial(kernel, n), out_shape=jax.ShapeDtypeStru...]
where the time goes in v2:
time: 50.8 us; the launch traced here: 50.7 us
  Pallas kernels  49 us (96%)
  local copies, waits for them, and re-layouts  1.67 us (3%)
    pallas_call x1, Pallas kernels, fused_body(): pl.pallas_call(functools.partial(kernel, n), out_shape=jax.ShapeDtypeStru...  49 us
    unnamed x1, local copies, waits for them, and re-layouts  1.67 us

profile of v2, /device:TPU:0, one launch (start us, length us, event | category | flops | bytes accessed | tf_op | source)
XLA Modules:
  0.0 50.7 jit_solution(612188256559557622)
XLA Ops:
  0.0 49.0 %shard_map.73 = bf16[128,1024]{1,0:T(8,128)(2,1)} custom-call(bf16[128,1024]{1,0:T(8,128)(2,1)} %tok_hbm.1, f32[1,1024]{1,0:T(1,128)} %bitcast.3, s32[2,512]{1,0:T(2,128)} %bitcast.4, f32[2,512]{1,0:T(2,128)} %bitcast.5, bf16[1,1024,896]{2,1,0:T(8,128)(2,1)} %gate_hbm.1, bf16[1,1024,896]{2,1,0:T(8,128)(2,1)} %up_hbm.1, bf16[1,896,1024]{2,1,0:T(8,128)(2,1)} %down_hbm.1), custom_call_target="tpu_custom_call" | custom-call | tf_op jit(solution)/shard_map/pallas_call | solution.py:428
  49.0 1.7 %copy.9 = bf16[128,1024]{1,0:T(8,128)(2,1)} copy(bf16[128,1024]{1,0:T(8,128)(2,1)} %shard_map.73) | data formatting | bytes 524288

commit v3 on v2

--- a/solution.py
+++ b/solution.py
@@ -15,6 +15,7 @@
 RELAY, SEND, REDUCE, COMPUTE = range(4)
 UNITS = 2
 PIECES = 4
+PHASES = 1
 LINE = 4
 SPREAD = ((11, 5, 14, 7), (11, 1, 7, 13), (15, 3, 8, 14), (11, 8, 13, 11))
 GATHER = ((8, 11, 15, 1), (12, 14, 12, 11), (15, 12, 3, 3), (12, 5, 7, 1))
@@ -210,8 +211,11 @@
         branches[0]()
         return
     half = len(branches) // 2
-    pl.when(index < low + half)(lambda: choose(index, low, branches[:half]))
-    pl.when(index >= low + half)(lambda: choose(index, low + half, branches[half:]))
+    lax.cond(
+        index < low + half,
+        lambda: choose(index, low, branches[:half]),
+        lambda: choose(index, low + half, branches[half:]),
+    )
 
 
 def pick(index, values):
@@ -226,8 +230,9 @@
     for op in order:
         if op[0] == COMPUTE:
             before.append(current)
-            steps.append(op[1:4])
             current = []
+            if op[4] == 0:
+                steps.append(op[1:4])
         else:
             current.append(op)
     return before, steps, current
@@ -235,7 +240,7 @@
 
 def kernel(
     n, tok_hbm, gain_hbm, ids_hbm, weight_hbm, gate_hbm, up_hbm, down_hbm, out_ref,
-    tok, gain, ids, weight, both, down, buf, own_shares, shares, part, srecv, rrecv,
+    tok, gain, ids, weight, both, down, hidden, buf, own_shares, shares, part, srecv, rrecv,
     load_sem, w_s, w_r, sib_s, ag_s, rs_s, ag_r, ags_r, rss_r, rs_r,
 ):
     ep = lax.axis_index("ep")
@@ -260,6 +265,18 @@
         return pltpu.make_async_remote_copy(
             src_ref=src, dst_ref=dst, send_sem=send, recv_sem=recv, device_id=to, device_id_type=MESH
         )
+
+    barrier = pltpu.get_barrier_semaphore()
+    for k in range(1, 4):
+        pl.semaphore_signal(barrier, inc=1, device_id={"ep": (ep + k) % 4}, device_id_type=MESH)
+
+    @pl.when(z < n - 1)
+    def _():
+        pl.semaphore_signal(barrier, inc=1, device_id=toward[UP], device_id_type=MESH)
+
+    @pl.when(z > 0)
+    def _():
+        pl.semaphore_signal(barrier, inc=1, device_id=toward[DOWN], device_id_type=MESH)
 
     loads = [
         pltpu.make_async_copy(src, dst, load_sem.at[i])
@@ -277,18 +294,6 @@
     ]
     for load in loads:
         load.start()
-
-    barrier = pltpu.get_barrier_semaphore()
-    for k in range(1, 4):
-        pl.semaphore_signal(barrier, inc=1, device_id={"ep": (ep + k) % 4}, device_id_type=MESH)
-
-    @pl.when(z < n - 1)
-    def _():
-        pl.semaphore_signal(barrier, inc=1, device_id=toward[UP], device_id_type=MESH)
-
-    @pl.when(z > 0)
-    def _():
-        pl.semaphore_signal(barrier, inc=1, device_id=toward[DOWN], device_id_type=MESH)
 
     loads[0].wait()
     loads[1].wait()
@@ -352,12 +357,16 @@
                         rs_s, rs_r.at[yb, at, number], toward[edge],
                     ).start()
 
+    for k in range(1, 4):
+        share(k).start()
+    shares[ep] = own_shares[ep]
+
     plans = [split(order) for order in ORDER]
     steps = len(plans[0][1])
-    branches, waited = [], [set() for _ in plans]
+    branches, waited = [[] for _ in range(PHASES)], [set() for _ in plans]
     for here, (before, _, _) in enumerate(plans):
-        for ops in before:
-            branches.append(functools.partial(run, here, ops, waited[here]))
+        for slot, ops in enumerate(before):
+            branches[slot % PHASES].append(functools.partial(run, here, ops, waited[here]))
             waited[here] = waited[here] | {(op[1], op[2], op[3] // per) for op in ops if op[0] == REDUCE}
 
     def column(row):
@@ -366,27 +375,29 @@
     lane = lax.broadcasted_iota(jnp.int32, (8, rows), 1)
 
     def one(step, carry):
-        choose(z * steps + step, 0, branches)
+        choose(z * steps + step, 0, branches[0])
 
         @pl.when(step == 0)
         def _():
-            for k in range(1, 4):
-                share(k).start()
-            shares[ep] = own_shares[ep]
-            remote(own_shares.at[pl.ds(0, 3)], shares.at[pl.ds(0, 3)], w_s, w_r, sib).wait_recv()
             for load in loads[4:]:
                 load.wait()
 
-        row, at, unit = (
-            pick(z, [pick(step, [s[i] for s in plan[1]]) for plan in plans]) for i in range(3)
-        )
+        code = pick(z, [pick(step, [(s[0] * n + s[1]) * UNITS + s[2] for s in plan[1]]) for plan in plans])
+        row, at, unit = code // (n * UNITS), code // UNITS % n, code % UNITS
         yb = row_of(row)
         theirs = buf.at[pl.ds(first(yb, at, unit, 1 - c), per)]
         remote(theirs, theirs, sib_s, ags_r.at[yb, at, unit], sib).wait_recv()
         x = buf[pl.ds(first(yb, at, unit, 0), 2 * per)].reshape(2 * tall, width)
         mixed = jnp.dot(x, both[...], preferred_element_type=jnp.float32)
-        hidden = (jax.nn.silu(mixed[:, :inner]) * mixed[:, inner:]).astype(jnp.bfloat16)
-        product = jnp.dot(hidden, down[...], preferred_element_type=jnp.float32)
+        hidden[...] = (jax.nn.silu(mixed[:, :inner]) * mixed[:, inner:]).astype(jnp.bfloat16)
+        for later in branches[1:]:
+            choose(z * steps + step, 0, later)
+        product = jnp.dot(hidden[...], down[...], preferred_element_type=jnp.float32)
+
+        @pl.when(step == 0)
+        def _():
+            remote(own_shares.at[pl.ds(0, 3)], shares.at[pl.ds(0, 3)], w_s, w_r, sib).wait_recv()
+
         ours = [jnp.broadcast_to(shares[2 * yb + half, pl.ds(at, 1), :], (8, rows)) for half in range(2)]
         turned = [pltpu.roll(values, tall, 1) for values in ours]
         early = jnp.where(lane < tall, ours[0], turned[1])
@@ -437,6 +448,7 @@
             pltpu.VMEM((TOP_K, n * rows), jnp.float32),
             pltpu.VMEM((width, 2 * inner), bf16),
             pltpu.VMEM((inner, width), bf16),
+            pltpu.VMEM((2 * rows // UNITS, inner), bf16),
             pltpu.VMEM((2 * n * UNITS * 2 * per, short, width), bf16),
             pltpu.VMEM((experts, n, rows), jnp.float32),
             pltpu.VMEM((experts, n, rows), jnp.float32),

time: 50.8 us -> 49.1 us (0.967)
  Pallas kernels: 49 us -> 47.3 us
    pallas_call x1, Pallas kernels: 49 us -> 47.3 us  [fused_body(): pl.pallas_call(functools.partial(kernel, n), out_shape=jax.ShapeDtypeStru...]
where the time goes in v3:
time: 49.1 us; the launch traced here: 49 us
  Pallas kernels  47.3 us (96%)
  local copies, waits for them, and re-layouts  1.67 us (3%)
    pallas_call x1, Pallas kernels, fused_body(): pl.pallas_call(functools.partial(kernel, n), out_shape=jax.ShapeDtypeStru...  47.3 us
    unnamed x1, local copies, waits for them, and re-layouts  1.67 us

profile of v3, /device:TPU:0, one launch (start us, length us, event | category | flops | bytes accessed | tf_op | source)
XLA Modules:
  0.0 49.0 jit_solution(1151391685262545767)
XLA Ops:
  0.0 47.3 %shard_map.73 = bf16[128,1024]{1,0:T(8,128)(2,1)} custom-call(bf16[128,1024]{1,0:T(8,128)(2,1)} %tok_hbm.1, f32[1,1024]{1,0:T(1,128)} %bitcast.3, s32[2,512]{1,0:T(2,128)} %bitcast.4, f32[2,512]{1,0:T(2,128)} %bitcast.5, bf16[1,1024,896]{2,1,0:T(8,128)(2,1)} %gate_hbm.1, bf16[1,1024,896]{2,1,0:T(8,128)(2,1)} %up_hbm.1, bf16[1,896,1024]{2,1,0:T(8,128)(2,1)} %down_hbm.1), custom_call_target="tpu_custom_call" | custom-call | tf_op jit(solution)/shard_map/pallas_call | solution.py:439
  47.3 1.7 %copy.9 = bf16[128,1024]{1,0:T(8,128)(2,1)} copy(bf16[128,1024]{1,0:T(8,128)(2,1)} %shard_map.73) | data formatting | bytes 524288

commit v4 on v3

--- a/solution.py
+++ b/solution.py
@@ -17,90 +17,90 @@
 PIECES = 4
 PHASES = 1
 LINE = 4
-SPREAD = ((11, 5, 14, 7), (11, 1, 7, 13), (15, 3, 8, 14), (11, 8, 13, 11))
-GATHER = ((8, 11, 15, 1), (12, 14, 12, 11), (15, 12, 3, 3), (12, 5, 7, 1))
+SPREAD = ((15, 5, 13, 11), (1, 3, 7, 15), (7, 7, 13, 14), (10, 12, 11, 10))
+GATHER = ((1, 11, 13, 1), (8, 14, 12, 15), (8, 15, 7, 11), (8, 7, 13, 11))
 ORDER = (
     (
-        (0, 0, 0, 0, 0), (0, 0, 0, 1, 0), (0, 0, 0, 2, 0), (0, 0, 0, 3, 0), (1, 0, 0, 0, 1), (1, 0, 0, 3, 0),
-        (1, 0, 0, 1, 1), (1, 0, 0, 0, 0), (3, 0, 0, 0, 0), (1, 0, 0, 3, 1), (1, 0, 0, 1, 0), (3, 0, 0, 1, 0),
-        (1, 0, 0, 2, 1), (0, 1, 0, 3, 0), (0, 0, 1, 3, 0), (1, 0, 1, 3, 0), (0, 1, 0, 0, 0), (0, 0, 1, 2, 0),
-        (1, 0, 1, 2, 0), (0, 1, 0, 1, 0), (1, 1, 0, 1, 1), (3, 0, 1, 1, 0), (0, 0, 1, 1, 0), (0, 1, 1, 3, 0),
-        (1, 0, 1, 1, 0), (1, 1, 1, 3, 1), (3, 1, 0, 0, 0), (2, 0, 1, 2, 1), (0, 0, 2, 2, 0), (0, 1, 1, 2, 0),
-        (0, 0, 1, 0, 0), (1, 0, 1, 0, 0), (2, 1, 0, 0, 1), (2, 1, 0, 1, 0), (3, 1, 1, 1, 0), (0, 1, 1, 1, 0),
-        (0, 0, 2, 0, 0), (1, 1, 1, 1, 1), (1, 0, 2, 0, 0), (3, 0, 1, 0, 0), (2, 1, 1, 2, 1), (2, 1, 1, 3, 0),
-        (0, 0, 2, 1, 0), (0, 1, 1, 0, 0), (2, 0, 1, 1, 1), (0, 0, 3, 0, 0), (3, 0, 2, 0, 0), (2, 0, 1, 0, 1),
-        (1, 0, 3, 0, 0), (3, 1, 1, 0, 0), (0, 0, 3, 2, 0), (0, 1, 2, 0, 0), (2, 0, 2, 1, 1), (1, 0, 2, 1, 0),
-        (0, 0, 3, 3, 0), (1, 0, 3, 3, 0), (2, 1, 1, 1, 1), (3, 0, 3, 1, 0), (0, 1, 0, 2, 0), (0, 1, 3, 0, 0),
-        (1, 0, 3, 2, 0), (2, 0, 1, 3, 1), (0, 1, 3, 1, 0), (0, 1, 2, 1, 0), (3, 1, 0, 1, 0), (0, 0, 3, 1, 0),
-        (2, 1, 1, 0, 1), (3, 1, 3, 0, 0), (2, 1, 0, 2, 0), (0, 0, 2, 3, 0), (0, 1, 3, 3, 0), (3, 1, 2, 0, 0),
-        (2, 1, 3, 0, 1), (2, 1, 3, 1, 0), (0, 1, 2, 2, 0), (0, 1, 3, 2, 0), (3, 0, 3, 0, 0), (2, 1, 2, 0, 0),
-        (2, 1, 2, 1, 1), (0, 1, 2, 3, 0), (3, 1, 3, 1, 0), (2, 0, 3, 0, 1), (3, 0, 2, 1, 0), (2, 0, 3, 1, 1),
-        (2, 1, 3, 2, 0), (3, 1, 2, 1, 0), (2, 0, 2, 0, 1), (2, 1, 3, 3, 0), (2, 1, 2, 3, 0), (2, 1, 2, 2, 0),
-        (2, 0, 3, 2, 1), (2, 0, 3, 3, 1), (2, 0, 2, 3, 1), (2, 1, 0, 3, 0), (2, 0, 2, 2, 1), (2, 0, 0, 1, 0),
-        (2, 0, 0, 3, 0), (2, 0, 0, 2, 0), (2, 0, 0, 0, 0),
+        (0, 0, 0, 0, 0), (0, 0, 0, 1, 0), (0, 0, 0, 2, 0), (0, 0, 0, 3, 0), (1, 0, 0, 1, 1), (1, 0, 0, 1, 0),
+        (1, 0, 0, 0, 1), (1, 0, 0, 0, 0), (3, 0, 0, 0, 0), (1, 0, 0, 2, 1), (1, 0, 0, 3, 0), (3, 0, 0, 1, 0),
+        (1, 0, 0, 3, 1), (1, 0, 0, 2, 0), (0, 1, 0, 1, 0), (0, 0, 1, 0, 0), (1, 1, 0, 1, 1), (1, 0, 1, 0, 0),
+        (0, 1, 0, 0, 0), (0, 0, 1, 1, 0), (3, 1, 0, 0, 0), (0, 1, 0, 3, 0), (1, 0, 1, 1, 0), (3, 0, 1, 0, 0),
+        (0, 0, 1, 2, 0), (0, 1, 0, 2, 0), (1, 1, 0, 2, 1), (1, 0, 1, 2, 0), (0, 0, 1, 3, 0), (1, 0, 1, 3, 0),
+        (0, 1, 1, 0, 0), (1, 1, 1, 0, 1), (3, 1, 0, 1, 0), (0, 0, 2, 1, 0), (0, 1, 1, 1, 0), (2, 0, 1, 0, 1),
+        (2, 1, 0, 1, 0), (3, 0, 1, 1, 0), (0, 0, 2, 0, 0), (0, 1, 1, 2, 0), (2, 0, 1, 1, 1), (1, 0, 2, 1, 0),
+        (3, 1, 1, 0, 0), (0, 0, 3, 0, 0), (2, 0, 1, 2, 1), (0, 1, 1, 3, 0), (1, 0, 2, 0, 0), (3, 0, 2, 0, 0),
+        (0, 0, 2, 2, 0), (2, 1, 1, 0, 1), (1, 0, 2, 2, 0), (3, 1, 1, 1, 0), (0, 0, 3, 2, 0), (2, 0, 2, 0, 1),
+        (1, 0, 3, 2, 0), (0, 1, 2, 1, 0), (0, 1, 3, 0, 0), (2, 1, 1, 1, 1), (2, 1, 1, 3, 0), (0, 1, 2, 0, 0),
+        (0, 1, 3, 1, 0), (2, 1, 1, 2, 1), (3, 1, 2, 0, 0), (0, 1, 2, 2, 0), (3, 1, 3, 0, 0), (0, 0, 3, 1, 0),
+        (0, 1, 3, 2, 0), (2, 1, 2, 0, 1), (2, 1, 2, 1, 0), (0, 1, 3, 3, 0), (2, 0, 1, 3, 1), (3, 0, 3, 0, 0),
+        (0, 0, 3, 3, 0), (2, 1, 3, 1, 0), (2, 1, 3, 0, 1), (3, 1, 3, 1, 0), (0, 0, 2, 3, 0), (2, 0, 2, 1, 1),
+        (3, 0, 3, 1, 0), (0, 1, 2, 3, 0), (2, 1, 3, 3, 0), (2, 0, 3, 0, 1), (3, 0, 2, 1, 0), (2, 1, 3, 2, 0),
+        (2, 0, 3, 1, 1), (3, 1, 2, 1, 0), (2, 1, 0, 2, 0), (2, 0, 3, 3, 1), (2, 1, 2, 2, 0), (2, 1, 2, 3, 0),
+        (2, 0, 3, 2, 1), (2, 0, 2, 2, 1), (2, 1, 0, 0, 0), (2, 0, 2, 3, 1), (2, 1, 0, 3, 0), (2, 0, 0, 1, 0),
+        (2, 0, 0, 0, 0), (2, 0, 0, 2, 0), (2, 0, 0, 3, 0),
     ),
     (
-        (0, 0, 1, 1, 0), (0, 0, 1, 0, 0), (0, 0, 1, 2, 0), (0, 0, 1, 3, 0), (1, 0, 1, 3, 1), (1, 0, 1, 3, 2),
-        (1, 0, 1, 0, 0), (1, 0, 1, 2, 1), (1, 0, 1, 2, 2), (1, 0, 1, 2, 0), (3, 0, 1, 0, 0), (1, 0, 1, 1, 2),
-        (1, 0, 1, 0, 1), (3, 0, 1, 1, 0), (0, 0, 0, 0, 0), (0, 0, 2, 2, 0), (1, 0, 0, 0, 0), (0, 1, 1, 0, 0),
-        (1, 0, 2, 2, 2), (1, 0, 0, 0, 1), (0, 0, 0, 1, 0), (1, 0, 0, 1, 1), (1, 0, 1, 0, 2), (0, 0, 2, 0, 0),
-        (1, 0, 2, 0, 0), (0, 1, 1, 2, 0), (3, 0, 0, 0, 0), (0, 0, 0, 3, 0), (1, 0, 0, 3, 0), (1, 0, 0, 3, 1),
-        (1, 0, 2, 0, 2), (0, 0, 2, 1, 0), (1, 0, 2, 1, 0), (0, 0, 0, 2, 0), (0, 1, 0, 0, 0), (1, 0, 0, 2, 1),
-        (1, 0, 2, 1, 2), (3, 0, 2, 0, 0), (0, 0, 3, 0, 0), (0, 1, 2, 0, 0), (0, 1, 0, 1, 0), (1, 0, 0, 2, 0),
-        (3, 0, 0, 1, 0), (0, 0, 2, 3, 0), (0, 1, 0, 3, 0), (1, 0, 3, 0, 2), (1, 0, 3, 0, 0), (1, 1, 0, 0, 1),
-        (3, 1, 0, 0, 0), (0, 0, 3, 2, 0), (0, 1, 2, 1, 0), (0, 1, 1, 3, 0), (1, 0, 3, 2, 2), (1, 0, 2, 3, 0),
-        (1, 1, 2, 1, 1), (3, 0, 2, 1, 0), (0, 0, 3, 3, 0), (0, 1, 0, 2, 0), (1, 0, 3, 3, 2), (3, 1, 2, 0, 0),
-        (2, 1, 0, 0, 1), (0, 0, 3, 1, 0), (0, 1, 3, 0, 0), (1, 1, 0, 2, 2), (1, 0, 1, 1, 1), (3, 0, 3, 1, 0),
-        (2, 1, 2, 0, 0), (0, 1, 1, 1, 0), (0, 1, 2, 3, 0), (0, 1, 3, 1, 0), (1, 1, 3, 1, 2), (1, 1, 1, 1, 1),
-        (1, 0, 3, 3, 0), (3, 1, 0, 1, 0), (0, 1, 3, 2, 0), (1, 0, 3, 1, 2), (3, 1, 3, 0, 0), (1, 0, 2, 3, 2),
-        (1, 1, 1, 0, 1), (2, 1, 0, 2, 0), (0, 1, 2, 2, 0), (3, 0, 3, 0, 0), (2, 1, 3, 1, 1), (1, 1, 2, 2, 2),
-        (3, 1, 1, 0, 0), (0, 1, 3, 3, 0), (1, 1, 2, 3, 2), (3, 1, 1, 1, 0), (2, 0, 2, 1, 1), (3, 1, 3, 1, 0),
-        (2, 1, 1, 1, 0), (2, 1, 1, 2, 1), (2, 1, 1, 3, 0), (3, 1, 2, 1, 0), (2, 1, 3, 2, 0), (2, 1, 3, 3, 2),
-        (2, 1, 1, 0, 1), (2, 1, 0, 1, 0), (2, 1, 3, 0, 1), (2, 1, 2, 3, 0), (2, 1, 2, 1, 1), (2, 1, 2, 2, 0),
-        (2, 0, 0, 3, 2), (2, 0, 3, 0, 1), (2, 1, 0, 3, 2), (2, 0, 3, 1, 1), (2, 0, 2, 0, 1), (2, 0, 0, 1, 2),
-        (2, 0, 3, 2, 1), (2, 0, 0, 2, 2), (2, 0, 3, 3, 1), (2, 0, 0, 0, 2), (2, 0, 2, 3, 1), (2, 0, 1, 2, 0),
-        (2, 0, 2, 2, 1), (2, 0, 1, 3, 0), (2, 0, 1, 1, 0), (2, 0, 1, 0, 0),
+        (0, 0, 1, 0, 0), (0, 0, 1, 1, 0), (0, 0, 1, 2, 0), (0, 0, 1, 3, 0), (1, 0, 1, 1, 0), (1, 0, 1, 0, 2),
+        (1, 0, 1, 3, 1), (1, 0, 1, 2, 0), (1, 0, 1, 1, 2), (1, 0, 1, 1, 1), (3, 0, 1, 0, 0), (1, 0, 1, 2, 2),
+        (1, 0, 1, 0, 1), (1, 0, 1, 3, 0), (3, 0, 1, 1, 0), (0, 0, 0, 1, 0), (0, 1, 1, 1, 0), (1, 0, 0, 1, 1),
+        (1, 0, 1, 3, 2), (0, 0, 2, 1, 0), (1, 0, 2, 1, 0), (0, 0, 0, 0, 0), (1, 0, 0, 0, 0), (0, 1, 1, 2, 0),
+        (1, 0, 2, 1, 2), (1, 0, 0, 0, 1), (3, 0, 0, 0, 0), (0, 0, 0, 2, 0), (0, 0, 2, 0, 0), (1, 0, 2, 0, 0),
+        (0, 1, 1, 3, 0), (1, 0, 2, 0, 2), (1, 0, 0, 2, 1), (0, 0, 2, 2, 0), (0, 0, 0, 3, 0), (3, 0, 2, 0, 0),
+        (0, 0, 3, 0, 0), (0, 1, 0, 1, 0), (0, 1, 2, 1, 0), (1, 0, 3, 0, 0), (1, 0, 3, 0, 2), (1, 0, 0, 3, 1),
+        (3, 1, 1, 1, 0), (0, 1, 0, 0, 0), (0, 1, 2, 2, 0), (1, 0, 2, 2, 2), (1, 0, 1, 2, 1), (1, 0, 0, 3, 0),
+        (3, 0, 0, 1, 0), (0, 0, 3, 2, 0), (0, 1, 0, 2, 0), (0, 1, 2, 0, 0), (1, 0, 3, 2, 0), (1, 1, 1, 1, 1),
+        (1, 0, 3, 2, 2), (3, 1, 0, 0, 0), (0, 0, 3, 3, 0), (0, 1, 1, 0, 0), (0, 1, 3, 0, 0), (1, 1, 3, 0, 2),
+        (1, 1, 1, 0, 1), (1, 0, 3, 3, 0), (3, 1, 2, 0, 0), (0, 1, 0, 3, 0), (0, 1, 3, 1, 0), (1, 1, 0, 3, 1),
+        (1, 1, 3, 1, 2), (2, 1, 1, 3, 0), (3, 0, 3, 1, 0), (0, 0, 3, 1, 0), (0, 1, 3, 2, 0), (1, 0, 3, 1, 2),
+        (2, 1, 2, 1, 0), (3, 1, 3, 0, 0), (0, 0, 2, 3, 0), (0, 1, 3, 3, 0), (1, 1, 3, 3, 2), (1, 0, 2, 3, 0),
+        (3, 1, 1, 0, 0), (2, 1, 3, 1, 0), (1, 0, 3, 3, 2), (3, 1, 3, 1, 0), (2, 1, 1, 0, 1), (1, 0, 2, 3, 2),
+        (3, 0, 2, 1, 0), (2, 1, 3, 3, 0), (2, 0, 2, 0, 1), (0, 1, 2, 3, 0), (1, 1, 2, 3, 2), (3, 1, 0, 1, 0),
+        (2, 1, 1, 1, 0), (2, 1, 3, 2, 1), (3, 1, 2, 1, 0), (2, 1, 1, 2, 1), (2, 1, 0, 2, 2), (3, 0, 3, 0, 0),
+        (2, 1, 2, 3, 0), (2, 1, 2, 0, 1), (2, 1, 2, 2, 0), (2, 0, 0, 0, 2), (2, 1, 0, 1, 0), (2, 1, 3, 0, 1),
+        (2, 0, 2, 1, 1), (2, 0, 0, 3, 2), (2, 0, 3, 0, 1), (2, 1, 0, 0, 2), (2, 0, 3, 1, 1), (2, 1, 0, 3, 2),
+        (2, 0, 3, 3, 1), (2, 0, 0, 1, 2), (2, 0, 3, 2, 1), (2, 0, 0, 2, 2), (2, 0, 1, 1, 0), (2, 0, 2, 2, 1),
+        (2, 0, 1, 2, 0), (2, 0, 2, 3, 1), (2, 0, 1, 3, 0), (2, 0, 1, 0, 0),
     ),
     (
-        (1, 0, 2, 2, 2), (0, 0, 2, 2, 0), (0, 0, 2, 1, 0), (0, 0, 2, 0, 0), (0, 0, 2, 3, 0), (1, 0, 2, 2, 1),
-        (1, 0, 2, 3, 0), (1, 0, 2, 0, 2), (1, 0, 2, 1, 1), (1, 0, 2, 0, 0), (3, 0, 2, 0, 0), (1, 0, 2, 0, 1),
-        (1, 0, 2, 1, 2), (3, 0, 2, 1, 0), (0, 0, 3, 0, 0), (0, 0, 1, 3, 0), (0, 1, 2, 3, 0), (1, 0, 1, 3, 0),
-        (1, 0, 3, 0, 2), (1, 0, 1, 3, 1), (1, 0, 2, 3, 2), (1, 0, 2, 3, 1), (0, 0, 1, 2, 0), (1, 0, 1, 2, 0),
-        (0, 0, 3, 2, 0), (0, 1, 2, 0, 0), (1, 0, 3, 2, 0), (1, 0, 3, 2, 2), (3, 0, 1, 1, 0), (0, 0, 3, 3, 0),
-        (0, 0, 1, 0, 0), (0, 1, 1, 3, 0), (1, 0, 1, 2, 1), (1, 0, 3, 3, 2), (1, 0, 1, 0, 1), (0, 0, 0, 0, 0),
-        (0, 0, 3, 1, 0), (3, 0, 3, 1, 0), (0, 0, 0, 1, 0), (0, 1, 1, 2, 0), (0, 1, 3, 3, 0), (1, 0, 0, 0, 1),
-        (1, 0, 0, 1, 0), (1, 0, 3, 1, 2), (3, 0, 3, 0, 0), (0, 0, 0, 3, 0), (0, 1, 3, 2, 0), (0, 1, 3, 1, 0),
-        (1, 0, 0, 3, 0), (1, 1, 3, 1, 2), (1, 0, 0, 3, 1), (3, 0, 0, 0, 0), (0, 0, 0, 2, 0), (1, 0, 0, 2, 1),
-        (1, 1, 3, 2, 2), (0, 1, 3, 0, 0), (1, 0, 0, 2, 0), (3, 1, 3, 1, 0), (0, 1, 0, 1, 0), (0, 1, 0, 0, 0),
-        (1, 1, 0, 1, 1), (3, 0, 0, 1, 0), (0, 1, 2, 2, 0), (0, 1, 0, 3, 0), (1, 1, 2, 2, 2), (3, 1, 3, 0, 0),
-        (0, 1, 2, 1, 0), (0, 1, 0, 2, 0), (1, 1, 0, 3, 1), (3, 1, 1, 1, 0), (2, 1, 3, 2, 0), (1, 0, 0, 1, 1),
-        (3, 1, 0, 0, 0), (2, 1, 1, 3, 2), (1, 1, 1, 2, 1), (3, 1, 0, 1, 0), (2, 1, 0, 1, 2), (2, 1, 0, 0, 1),
-        (0, 0, 1, 1, 0), (3, 1, 2, 1, 0), (2, 1, 0, 2, 0), (2, 1, 3, 3, 2), (0, 1, 1, 1, 0), (1, 1, 1, 1, 1),
-        (3, 0, 1, 0, 0), (2, 1, 2, 3, 2), (0, 1, 1, 0, 0), (1, 0, 1, 1, 1), (3, 1, 2, 0, 0), (2, 1, 2, 2, 2),
-        (2, 1, 3, 1, 0), (1, 1, 2, 1, 1), (3, 1, 1, 0, 0), (2, 1, 2, 0, 0), (2, 0, 0, 3, 2), (2, 1, 1, 2, 0),
-        (2, 1, 1, 1, 0), (2, 1, 0, 3, 2), (2, 1, 1, 0, 0), (2, 0, 0, 1, 2), (2, 1, 3, 0, 0), (2, 0, 0, 2, 2),
-        (2, 1, 2, 1, 0), (2, 0, 0, 0, 2), (2, 0, 1, 2, 2), (2, 0, 3, 0, 1), (2, 0, 3, 1, 1), (2, 0, 1, 3, 2),
-        (2, 0, 1, 1, 2), (2, 0, 3, 2, 1), (2, 0, 1, 0, 2), (2, 0, 3, 3, 1), (2, 0, 2, 1, 0), (2, 0, 2, 3, 0),
-        (2, 0, 2, 0, 0), (2, 0, 2, 2, 0),
+        (0, 0, 2, 0, 0), (0, 0, 2, 1, 0), (0, 0, 2, 2, 0), (0, 0, 2, 3, 0), (1, 0, 2, 1, 2), (1, 0, 2, 2, 1),
+        (1, 0, 2, 2, 0), (1, 0, 2, 0, 2), (1, 0, 2, 3, 1), (1, 0, 2, 3, 0), (3, 0, 2, 0, 0), (1, 0, 2, 2, 2),
+        (1, 0, 2, 1, 1), (1, 0, 2, 0, 0), (3, 0, 2, 1, 0), (0, 0, 3, 0, 0), (0, 0, 1, 3, 0), (0, 1, 2, 2, 0),
+        (1, 0, 3, 0, 2), (1, 0, 1, 3, 0), (1, 0, 1, 3, 1), (0, 0, 1, 1, 0), (1, 1, 2, 2, 2), (0, 0, 3, 1, 0),
+        (1, 0, 3, 1, 0), (0, 1, 2, 3, 0), (1, 0, 1, 1, 1), (3, 0, 3, 0, 0), (0, 0, 3, 2, 0), (0, 0, 1, 0, 0),
+        (0, 1, 2, 0, 0), (1, 0, 3, 2, 2), (1, 0, 1, 0, 1), (1, 0, 2, 1, 0), (3, 1, 2, 1, 0), (0, 0, 3, 3, 0),
+        (0, 0, 0, 1, 0), (0, 1, 1, 3, 0), (1, 0, 0, 1, 0), (1, 0, 3, 3, 2), (1, 0, 0, 1, 1), (3, 0, 1, 0, 0),
+        (0, 0, 0, 0, 0), (0, 1, 3, 1, 0), (0, 1, 3, 2, 0), (1, 0, 0, 0, 0), (1, 1, 3, 1, 2), (1, 0, 0, 0, 1),
+        (3, 0, 3, 1, 0), (0, 0, 0, 2, 0), (0, 1, 2, 1, 0), (0, 1, 3, 3, 0), (1, 0, 0, 2, 1), (1, 0, 0, 2, 0),
+        (1, 0, 3, 1, 2), (3, 0, 0, 0, 0), (0, 0, 0, 3, 0), (0, 1, 0, 1, 0), (0, 1, 3, 0, 0), (1, 0, 0, 3, 1),
+        (1, 0, 2, 3, 2), (3, 1, 3, 1, 0), (0, 0, 1, 2, 0), (0, 1, 0, 0, 0), (1, 0, 1, 2, 0), (1, 1, 0, 1, 1),
+        (2, 1, 2, 3, 2), (3, 1, 2, 0, 0), (0, 1, 1, 1, 0), (0, 1, 0, 2, 0), (1, 1, 1, 1, 1), (3, 0, 1, 1, 0),
+        (0, 1, 1, 0, 0), (2, 1, 2, 1, 0), (1, 1, 1, 0, 1), (3, 1, 0, 0, 0), (0, 1, 1, 2, 0), (0, 1, 0, 3, 0),
+        (1, 1, 1, 2, 1), (3, 0, 0, 1, 0), (3, 1, 3, 0, 0), (2, 1, 0, 1, 2), (1, 0, 1, 2, 1), (2, 1, 2, 2, 0),
+        (3, 1, 1, 1, 0), (2, 1, 3, 1, 0), (1, 1, 2, 1, 1), (2, 0, 0, 0, 2), (3, 1, 1, 0, 0), (2, 1, 1, 3, 0),
+        (1, 1, 2, 0, 1), (3, 1, 0, 1, 0), (2, 1, 1, 1, 0), (2, 1, 1, 0, 1), (2, 0, 0, 3, 2), (2, 1, 3, 3, 1),
+        (2, 1, 0, 0, 2), (2, 1, 3, 2, 0), (1, 0, 2, 0, 1), (2, 1, 0, 2, 0), (2, 1, 0, 3, 2), (2, 1, 1, 2, 0),
+        (2, 1, 2, 0, 1), (2, 0, 0, 1, 2), (2, 1, 3, 0, 1), (2, 0, 0, 2, 2), (2, 0, 1, 1, 2), (2, 0, 3, 0, 1),
+        (2, 0, 1, 2, 2), (2, 0, 3, 1, 1), (2, 0, 1, 3, 2), (2, 0, 3, 3, 1), (2, 0, 1, 0, 2), (2, 0, 3, 2, 1),
+        (2, 0, 2, 1, 0), (2, 0, 2, 2, 0), (2, 0, 2, 0, 0), (2, 0, 2, 3, 0),
     ),
     (
-        (0, 0, 3, 0, 0), (0, 0, 3, 1, 0), (0, 0, 3, 2, 0), (0, 0, 3, 3, 0), (1, 0, 3, 0, 2), (1, 0, 3, 3, 0),
-        (1, 0, 3, 2, 2), (1, 0, 3, 1, 0), (3, 0, 3, 0, 0), (1, 0, 3, 3, 2), (1, 0, 3, 0, 0), (3, 0, 3, 1, 0),
-        (1, 0, 3, 1, 2), (1, 0, 3, 2, 0), (0, 0, 2, 2, 0), (0, 1, 3, 3, 0), (1, 1, 3, 3, 2), (1, 0, 2, 2, 0),
-        (0, 1, 3, 1, 0), (0, 0, 2, 1, 0), (1, 1, 3, 1, 2), (0, 0, 2, 0, 0), (0, 1, 3, 0, 0), (1, 0, 2, 0, 0),
-        (1, 1, 3, 0, 2), (3, 0, 2, 0, 0), (0, 0, 1, 3, 0), (0, 1, 3, 2, 0), (1, 0, 1, 3, 0), (3, 1, 3, 0, 0),
-        (0, 1, 2, 2, 0), (0, 0, 2, 3, 0), (1, 0, 2, 3, 0), (1, 1, 2, 2, 2), (3, 1, 3, 1, 0), (2, 1, 3, 0, 0),
-        (2, 1, 3, 1, 2), (0, 0, 1, 2, 0), (0, 1, 2, 0, 0), (3, 0, 2, 1, 0), (2, 1, 3, 2, 2), (0, 0, 1, 0, 0),
-        (0, 1, 1, 3, 0), (1, 0, 1, 0, 0), (3, 0, 1, 1, 0), (2, 0, 2, 3, 2), (0, 0, 0, 0, 0), (0, 1, 2, 3, 0),
-        (1, 0, 0, 0, 0), (2, 0, 2, 2, 2), (0, 0, 0, 3, 0), (3, 1, 2, 1, 0), (2, 1, 3, 3, 2), (0, 0, 0, 2, 0),
-        (1, 0, 0, 2, 0), (0, 1, 1, 0, 0), (2, 1, 2, 3, 2), (3, 0, 0, 1, 0), (0, 1, 0, 0, 0), (0, 1, 0, 1, 0),
-        (2, 1, 2, 2, 2), (0, 1, 0, 3, 0), (0, 1, 0, 2, 0), (3, 1, 0, 0, 0), (2, 0, 0, 3, 2), (0, 0, 0, 1, 0),
-        (3, 1, 0, 1, 0), (2, 1, 0, 1, 0), (0, 1, 1, 2, 0), (3, 0, 0, 0, 0), (2, 1, 0, 2, 0), (2, 1, 0, 3, 2),
-        (3, 1, 1, 1, 0), (2, 1, 0, 0, 0), (0, 1, 1, 1, 0), (2, 0, 0, 1, 2), (2, 1, 1, 2, 0), (3, 1, 1, 0, 0),
-        (2, 1, 1, 3, 0), (2, 0, 0, 2, 2), (0, 0, 1, 1, 0), (0, 1, 2, 1, 0), (2, 1, 1, 1, 0), (2, 0, 0, 0, 2),
-        (3, 0, 1, 0, 0), (2, 1, 1, 0, 0), (2, 0, 1, 2, 2), (3, 1, 2, 0, 0), (2, 0, 1, 3, 2), (2, 1, 2, 1, 0),
-        (2, 1, 2, 0, 0), (2, 0, 1, 1, 2), (2, 0, 1, 0, 2), (2, 0, 2, 1, 2), (2, 0, 2, 0, 2), (2, 0, 3, 0, 0),
-        (2, 0, 3, 1, 0), (2, 0, 3, 2, 0), (2, 0, 3, 3, 0),
+        (0, 0, 3, 0, 0), (0, 0, 3, 1, 0), (0, 0, 3, 2, 0), (0, 0, 3, 3, 0), (1, 0, 3, 0, 2), (1, 0, 3, 2, 0),
+        (1, 0, 3, 1, 2), (1, 0, 3, 1, 0), (3, 0, 3, 0, 0), (1, 0, 3, 3, 0), (1, 0, 3, 2, 2), (3, 0, 3, 1, 0),
+        (1, 0, 3, 3, 2), (1, 0, 3, 0, 0), (0, 0, 2, 2, 0), (0, 1, 3, 2, 0), (1, 1, 3, 2, 2), (1, 0, 2, 2, 0),
+        (0, 0, 2, 3, 0), (0, 1, 3, 1, 0), (3, 0, 2, 1, 0), (0, 1, 3, 3, 0), (0, 0, 2, 1, 0), (1, 0, 2, 3, 0),
+        (1, 1, 3, 3, 2), (0, 0, 1, 3, 0), (0, 1, 3, 0, 0), (1, 0, 1, 3, 0), (1, 1, 3, 0, 2), (3, 1, 3, 1, 0),
+        (0, 0, 1, 1, 0), (0, 1, 2, 2, 0), (2, 0, 2, 2, 2), (3, 1, 3, 0, 0), (0, 0, 1, 0, 0), (0, 1, 2, 3, 0),
+        (2, 1, 3, 2, 0), (3, 0, 1, 0, 0), (0, 0, 0, 1, 0), (0, 1, 1, 3, 0), (2, 1, 3, 1, 2), (3, 1, 2, 1, 0),
+        (0, 0, 0, 0, 0), (1, 0, 0, 0, 0), (0, 0, 0, 2, 0), (1, 0, 0, 2, 0), (3, 0, 0, 0, 0), (0, 0, 0, 3, 0),
+        (1, 0, 0, 3, 0), (2, 1, 2, 2, 2), (2, 1, 2, 3, 0), (0, 1, 0, 0, 0), (2, 0, 0, 0, 2), (0, 1, 0, 1, 0),
+        (3, 0, 0, 1, 0), (3, 1, 0, 0, 0), (0, 1, 0, 2, 0), (0, 1, 1, 1, 0), (2, 0, 0, 3, 2), (0, 1, 0, 3, 0),
+        (0, 1, 1, 0, 0), (2, 1, 0, 0, 2), (2, 1, 0, 1, 0), (3, 1, 0, 1, 0), (0, 1, 1, 2, 0), (2, 0, 2, 3, 2),
+        (3, 1, 1, 0, 0), (0, 0, 1, 2, 0), (2, 1, 0, 2, 0), (2, 1, 0, 3, 2), (3, 1, 1, 1, 0), (0, 1, 2, 1, 0),
+        (2, 1, 1, 1, 0), (2, 0, 0, 1, 2), (3, 0, 1, 1, 0), (0, 1, 2, 0, 0), (2, 1, 1, 2, 0), (2, 1, 1, 3, 0),
+        (2, 0, 0, 2, 2), (3, 1, 2, 0, 0), (2, 0, 1, 1, 2), (2, 1, 1, 0, 0), (2, 1, 3, 3, 0), (2, 0, 1, 2, 2),
+        (0, 0, 2, 0, 0), (2, 1, 2, 1, 0), (2, 0, 1, 3, 2), (3, 0, 2, 0, 0), (2, 1, 2, 0, 0), (2, 0, 1, 0, 2),
+        (2, 1, 3, 0, 0), (2, 0, 2, 1, 2), (2, 0, 2, 0, 2), (2, 0, 3, 1, 0), (2, 0, 3, 0, 0), (2, 0, 3, 3, 0),
+        (2, 0, 3, 2, 0),
     ),
 )
 

time: 49.1 us -> 48.5 us (0.988)
  the two profiles are of different devices: /device:TPU:0 before, /device:TPU:18 now
where the time goes in v4:
time: 48.5 us; the launch traced here: 48.4 us
  Pallas kernels  46.7 us (96%)
  local copies, waits for them, and re-layouts  1.67 us (3%)
    pallas_call x1, Pallas kernels, fused_body(): pl.pallas_call(functools.partial(kernel, n), out_shape=jax.ShapeDtypeStru...  46.7 us
    unnamed x1, local copies, waits for them, and re-layouts  1.67 us

profile of v4, /device:TPU:18, one launch (start us, length us, event | category | flops | bytes accessed | tf_op | source)
XLA Modules:
  0.0 48.4 jit_solution(3933200431150006096)
XLA Ops:
  0.0 46.7 %shard_map.73 = bf16[128,1024]{1,0:T(8,128)(2,1)} custom-call(bf16[128,1024]{1,0:T(8,128)(2,1)} %tok_hbm.1, f32[1,1024]{1,0:T(1,128)} %bitcast.3, s32[2,512]{1,0:T(2,128)} %bitcast.4, f32[2,512]{1,0:T(2,128)} %bitcast.5, bf16[1,1024,896]{2,1,0:T(8,128)(2,1)} %gate_hbm.1, bf16[1,1024,896]{2,1,0:T(8,128)(2,1)} %up_hbm.1, bf16[1,896,1024]{2,1,0:T(8,128)(2,1)} %down_hbm.1), custom_call_target="tpu_custom_call" | custom-call | tf_op jit(solution)/shard_map/pallas_call | solution.py:439
  46.7 1.7 %copy.9 = bf16[128,1024]{1,0:T(8,128)(2,1)} copy(bf16[128,1024]{1,0:T(8,128)(2,1)} %shard_map.73) | data formatting | bytes 524288

commit v5 on v4

--- a/solution.py
+++ b/solution.py
@@ -17,90 +17,90 @@
 PIECES = 4
 PHASES = 1
 LINE = 4
-SPREAD = ((15, 5, 13, 11), (1, 3, 7, 15), (7, 7, 13, 14), (10, 12, 11, 10))
-GATHER = ((1, 11, 13, 1), (8, 14, 12, 15), (8, 15, 7, 11), (8, 7, 13, 11))
+SPREAD = ((1, 15, 15, 5), (8, 13, 15, 1), (13, 11, 14, 7), (8, 7, 13, 14))
+GATHER = ((15, 14, 14, 1), (1, 15, 15, 12), (7, 8, 15, 13), (8, 15, 8, 3))
 ORDER = (
     (
-        (0, 0, 0, 0, 0), (0, 0, 0, 1, 0), (0, 0, 0, 2, 0), (0, 0, 0, 3, 0), (1, 0, 0, 1, 1), (1, 0, 0, 1, 0),
-        (1, 0, 0, 0, 1), (1, 0, 0, 0, 0), (3, 0, 0, 0, 0), (1, 0, 0, 2, 1), (1, 0, 0, 3, 0), (3, 0, 0, 1, 0),
-        (1, 0, 0, 3, 1), (1, 0, 0, 2, 0), (0, 1, 0, 1, 0), (0, 0, 1, 0, 0), (1, 1, 0, 1, 1), (1, 0, 1, 0, 0),
-        (0, 1, 0, 0, 0), (0, 0, 1, 1, 0), (3, 1, 0, 0, 0), (0, 1, 0, 3, 0), (1, 0, 1, 1, 0), (3, 0, 1, 0, 0),
-        (0, 0, 1, 2, 0), (0, 1, 0, 2, 0), (1, 1, 0, 2, 1), (1, 0, 1, 2, 0), (0, 0, 1, 3, 0), (1, 0, 1, 3, 0),
-        (0, 1, 1, 0, 0), (1, 1, 1, 0, 1), (3, 1, 0, 1, 0), (0, 0, 2, 1, 0), (0, 1, 1, 1, 0), (2, 0, 1, 0, 1),
-        (2, 1, 0, 1, 0), (3, 0, 1, 1, 0), (0, 0, 2, 0, 0), (0, 1, 1, 2, 0), (2, 0, 1, 1, 1), (1, 0, 2, 1, 0),
-        (3, 1, 1, 0, 0), (0, 0, 3, 0, 0), (2, 0, 1, 2, 1), (0, 1, 1, 3, 0), (1, 0, 2, 0, 0), (3, 0, 2, 0, 0),
-        (0, 0, 2, 2, 0), (2, 1, 1, 0, 1), (1, 0, 2, 2, 0), (3, 1, 1, 1, 0), (0, 0, 3, 2, 0), (2, 0, 2, 0, 1),
-        (1, 0, 3, 2, 0), (0, 1, 2, 1, 0), (0, 1, 3, 0, 0), (2, 1, 1, 1, 1), (2, 1, 1, 3, 0), (0, 1, 2, 0, 0),
-        (0, 1, 3, 1, 0), (2, 1, 1, 2, 1), (3, 1, 2, 0, 0), (0, 1, 2, 2, 0), (3, 1, 3, 0, 0), (0, 0, 3, 1, 0),
-        (0, 1, 3, 2, 0), (2, 1, 2, 0, 1), (2, 1, 2, 1, 0), (0, 1, 3, 3, 0), (2, 0, 1, 3, 1), (3, 0, 3, 0, 0),
-        (0, 0, 3, 3, 0), (2, 1, 3, 1, 0), (2, 1, 3, 0, 1), (3, 1, 3, 1, 0), (0, 0, 2, 3, 0), (2, 0, 2, 1, 1),
-        (3, 0, 3, 1, 0), (0, 1, 2, 3, 0), (2, 1, 3, 3, 0), (2, 0, 3, 0, 1), (3, 0, 2, 1, 0), (2, 1, 3, 2, 0),
-        (2, 0, 3, 1, 1), (3, 1, 2, 1, 0), (2, 1, 0, 2, 0), (2, 0, 3, 3, 1), (2, 1, 2, 2, 0), (2, 1, 2, 3, 0),
-        (2, 0, 3, 2, 1), (2, 0, 2, 2, 1), (2, 1, 0, 0, 0), (2, 0, 2, 3, 1), (2, 1, 0, 3, 0), (2, 0, 0, 1, 0),
-        (2, 0, 0, 0, 0), (2, 0, 0, 2, 0), (2, 0, 0, 3, 0),
+        (0, 0, 0, 0, 0), (0, 0, 0, 1, 0), (0, 0, 0, 2, 0), (0, 0, 0, 3, 0), (1, 0, 0, 1, 0), (1, 0, 0, 1, 1),
+        (1, 0, 0, 0, 0), (1, 0, 0, 3, 1), (3, 0, 0, 0, 0), (1, 0, 0, 2, 0), (1, 0, 0, 2, 1), (3, 0, 0, 1, 0),
+        (0, 1, 0, 1, 0), (1, 0, 0, 3, 0), (1, 0, 0, 0, 1), (0, 0, 1, 3, 0), (0, 1, 0, 0, 0), (1, 0, 1, 3, 0),
+        (1, 1, 0, 0, 1), (0, 0, 1, 2, 0), (3, 1, 0, 0, 0), (0, 1, 0, 2, 0), (1, 0, 1, 2, 0), (3, 0, 1, 1, 0),
+        (0, 1, 0, 3, 0), (0, 0, 1, 0, 0), (2, 1, 0, 0, 0), (2, 1, 0, 1, 1), (0, 0, 1, 1, 0), (1, 1, 0, 3, 1),
+        (0, 1, 1, 3, 0), (1, 0, 1, 1, 0), (3, 1, 0, 1, 0), (0, 0, 2, 1, 0), (1, 1, 1, 3, 1), (0, 1, 1, 2, 0),
+        (1, 0, 2, 1, 0), (3, 0, 1, 0, 0), (3, 1, 1, 1, 0), (0, 0, 2, 0, 0), (1, 0, 2, 0, 0), (2, 0, 1, 3, 1),
+        (0, 0, 3, 3, 0), (0, 1, 1, 1, 0), (1, 1, 1, 1, 1), (3, 0, 2, 0, 0), (0, 0, 3, 2, 0), (0, 1, 2, 1, 0),
+        (1, 0, 3, 2, 0), (2, 1, 1, 3, 1), (2, 1, 1, 2, 0), (0, 0, 3, 1, 0), (3, 0, 3, 1, 0), (0, 1, 2, 0, 0),
+        (1, 0, 3, 1, 0), (2, 0, 2, 1, 1), (0, 1, 3, 3, 0), (2, 1, 0, 2, 1), (0, 1, 3, 2, 0), (3, 1, 2, 0, 0),
+        (0, 0, 2, 3, 0), (2, 0, 3, 2, 1), (1, 0, 2, 3, 0), (3, 1, 3, 1, 0), (0, 1, 2, 2, 0), (2, 1, 2, 1, 1),
+        (2, 1, 2, 0, 0), (0, 1, 3, 1, 0), (0, 1, 3, 0, 0), (2, 1, 3, 3, 0), (2, 1, 3, 2, 1), (0, 1, 2, 3, 0),
+        (3, 1, 3, 0, 0), (0, 0, 3, 0, 0), (2, 0, 1, 2, 1), (3, 1, 2, 1, 0), (0, 0, 2, 2, 0), (2, 1, 3, 0, 1),
+        (2, 1, 3, 1, 0), (3, 0, 3, 0, 0), (0, 1, 1, 0, 0), (2, 1, 2, 2, 0), (2, 0, 3, 3, 1), (3, 0, 2, 1, 0),
+        (2, 0, 3, 0, 1), (2, 1, 2, 3, 0), (3, 1, 1, 0, 0), (2, 0, 3, 1, 1), (2, 0, 2, 2, 1), (2, 1, 1, 1, 0),
+        (2, 0, 2, 3, 1), (2, 1, 1, 0, 0), (2, 0, 2, 0, 1), (2, 1, 0, 3, 0), (2, 0, 1, 1, 1), (2, 0, 0, 1, 0),
+        (2, 0, 1, 0, 1), (2, 0, 0, 0, 0), (2, 0, 0, 3, 0), (2, 0, 0, 2, 0),
     ),
     (
-        (0, 0, 1, 0, 0), (0, 0, 1, 1, 0), (0, 0, 1, 2, 0), (0, 0, 1, 3, 0), (1, 0, 1, 1, 0), (1, 0, 1, 0, 2),
-        (1, 0, 1, 3, 1), (1, 0, 1, 2, 0), (1, 0, 1, 1, 2), (1, 0, 1, 1, 1), (3, 0, 1, 0, 0), (1, 0, 1, 2, 2),
-        (1, 0, 1, 0, 1), (1, 0, 1, 3, 0), (3, 0, 1, 1, 0), (0, 0, 0, 1, 0), (0, 1, 1, 1, 0), (1, 0, 0, 1, 1),
-        (1, 0, 1, 3, 2), (0, 0, 2, 1, 0), (1, 0, 2, 1, 0), (0, 0, 0, 0, 0), (1, 0, 0, 0, 0), (0, 1, 1, 2, 0),
-        (1, 0, 2, 1, 2), (1, 0, 0, 0, 1), (3, 0, 0, 0, 0), (0, 0, 0, 2, 0), (0, 0, 2, 0, 0), (1, 0, 2, 0, 0),
-        (0, 1, 1, 3, 0), (1, 0, 2, 0, 2), (1, 0, 0, 2, 1), (0, 0, 2, 2, 0), (0, 0, 0, 3, 0), (3, 0, 2, 0, 0),
-        (0, 0, 3, 0, 0), (0, 1, 0, 1, 0), (0, 1, 2, 1, 0), (1, 0, 3, 0, 0), (1, 0, 3, 0, 2), (1, 0, 0, 3, 1),
-        (3, 1, 1, 1, 0), (0, 1, 0, 0, 0), (0, 1, 2, 2, 0), (1, 0, 2, 2, 2), (1, 0, 1, 2, 1), (1, 0, 0, 3, 0),
-        (3, 0, 0, 1, 0), (0, 0, 3, 2, 0), (0, 1, 0, 2, 0), (0, 1, 2, 0, 0), (1, 0, 3, 2, 0), (1, 1, 1, 1, 1),
-        (1, 0, 3, 2, 2), (3, 1, 0, 0, 0), (0, 0, 3, 3, 0), (0, 1, 1, 0, 0), (0, 1, 3, 0, 0), (1, 1, 3, 0, 2),
-        (1, 1, 1, 0, 1), (1, 0, 3, 3, 0), (3, 1, 2, 0, 0), (0, 1, 0, 3, 0), (0, 1, 3, 1, 0), (1, 1, 0, 3, 1),
-        (1, 1, 3, 1, 2), (2, 1, 1, 3, 0), (3, 0, 3, 1, 0), (0, 0, 3, 1, 0), (0, 1, 3, 2, 0), (1, 0, 3, 1, 2),
-        (2, 1, 2, 1, 0), (3, 1, 3, 0, 0), (0, 0, 2, 3, 0), (0, 1, 3, 3, 0), (1, 1, 3, 3, 2), (1, 0, 2, 3, 0),
-        (3, 1, 1, 0, 0), (2, 1, 3, 1, 0), (1, 0, 3, 3, 2), (3, 1, 3, 1, 0), (2, 1, 1, 0, 1), (1, 0, 2, 3, 2),
-        (3, 0, 2, 1, 0), (2, 1, 3, 3, 0), (2, 0, 2, 0, 1), (0, 1, 2, 3, 0), (1, 1, 2, 3, 2), (3, 1, 0, 1, 0),
-        (2, 1, 1, 1, 0), (2, 1, 3, 2, 1), (3, 1, 2, 1, 0), (2, 1, 1, 2, 1), (2, 1, 0, 2, 2), (3, 0, 3, 0, 0),
-        (2, 1, 2, 3, 0), (2, 1, 2, 0, 1), (2, 1, 2, 2, 0), (2, 0, 0, 0, 2), (2, 1, 0, 1, 0), (2, 1, 3, 0, 1),
-        (2, 0, 2, 1, 1), (2, 0, 0, 3, 2), (2, 0, 3, 0, 1), (2, 1, 0, 0, 2), (2, 0, 3, 1, 1), (2, 1, 0, 3, 2),
-        (2, 0, 3, 3, 1), (2, 0, 0, 1, 2), (2, 0, 3, 2, 1), (2, 0, 0, 2, 2), (2, 0, 1, 1, 0), (2, 0, 2, 2, 1),
-        (2, 0, 1, 2, 0), (2, 0, 2, 3, 1), (2, 0, 1, 3, 0), (2, 0, 1, 0, 0),
+        (0, 0, 1, 0, 0), (0, 0, 1, 3, 0), (0, 0, 1, 1, 0), (0, 0, 1, 2, 0), (1, 0, 1, 3, 2), (1, 0, 1, 0, 1),
+        (1, 0, 1, 2, 0), (1, 0, 1, 2, 2), (1, 0, 1, 1, 1), (3, 0, 1, 0, 0), (1, 0, 1, 0, 2), (1, 0, 1, 3, 1),
+        (3, 0, 1, 1, 0), (0, 0, 0, 1, 0), (1, 0, 0, 1, 0), (0, 1, 1, 2, 0), (1, 0, 0, 1, 1), (1, 0, 1, 1, 2),
+        (0, 0, 2, 1, 0), (0, 0, 0, 3, 0), (1, 0, 2, 1, 0), (1, 0, 2, 1, 2), (1, 0, 0, 3, 1), (0, 0, 2, 0, 0),
+        (0, 0, 0, 2, 0), (1, 0, 0, 2, 0), (3, 0, 2, 0, 0), (0, 0, 0, 0, 0), (0, 0, 2, 3, 0), (0, 1, 0, 1, 0),
+        (1, 0, 2, 3, 0), (1, 0, 0, 2, 1), (1, 0, 2, 0, 2), (3, 0, 0, 1, 0), (0, 0, 3, 3, 0), (0, 1, 0, 0, 0),
+        (0, 1, 2, 1, 0), (1, 1, 0, 0, 1), (1, 0, 3, 3, 0), (1, 0, 3, 3, 2), (3, 0, 0, 0, 0), (0, 0, 3, 2, 0),
+        (0, 1, 0, 2, 0), (1, 0, 3, 2, 2), (1, 0, 0, 0, 1), (3, 1, 0, 0, 0), (0, 0, 3, 1, 0), (0, 1, 2, 3, 0),
+        (1, 0, 3, 1, 2), (1, 0, 3, 1, 0), (1, 0, 1, 2, 1), (3, 0, 3, 1, 0), (0, 0, 2, 2, 0), (0, 1, 3, 3, 0),
+        (0, 1, 0, 3, 0), (1, 0, 2, 2, 0), (1, 1, 3, 3, 2), (1, 1, 2, 1, 1), (2, 1, 0, 0, 0), (0, 1, 3, 0, 0),
+        (0, 1, 1, 3, 0), (1, 1, 1, 3, 1), (1, 0, 2, 3, 2), (3, 0, 2, 1, 0), (0, 1, 3, 1, 0), (2, 1, 0, 1, 0),
+        (0, 1, 2, 0, 0), (3, 1, 1, 1, 0), (0, 1, 2, 2, 0), (1, 1, 2, 2, 2), (3, 1, 3, 0, 0), (0, 1, 1, 1, 0),
+        (0, 1, 3, 2, 0), (2, 1, 1, 2, 0), (1, 1, 3, 0, 2), (3, 1, 2, 0, 0), (0, 0, 3, 0, 0), (1, 0, 3, 0, 2),
+        (2, 1, 3, 1, 0), (2, 1, 1, 3, 1), (3, 1, 3, 1, 0), (0, 1, 1, 0, 0), (1, 0, 2, 2, 2), (2, 1, 2, 0, 0),
+        (2, 0, 2, 1, 1), (3, 0, 3, 0, 0), (2, 1, 3, 3, 0), (1, 1, 1, 0, 2), (3, 1, 0, 1, 0), (2, 0, 3, 2, 1),
+        (3, 1, 2, 1, 0), (2, 1, 2, 1, 1), (2, 1, 0, 2, 0), (3, 1, 1, 0, 0), (2, 1, 2, 3, 1), (2, 1, 2, 2, 0),
+        (2, 1, 3, 2, 1), (2, 0, 0, 3, 2), (2, 1, 1, 1, 0), (2, 1, 3, 0, 1), (2, 1, 1, 0, 2), (2, 0, 3, 3, 1),
+        (2, 1, 0, 3, 2), (2, 0, 3, 0, 1), (2, 0, 0, 1, 2), (2, 0, 3, 1, 1), (2, 0, 0, 0, 2), (2, 0, 2, 2, 1),
+        (2, 0, 0, 2, 2), (2, 0, 2, 3, 1), (2, 0, 2, 0, 1), (2, 0, 1, 2, 0), (2, 0, 1, 1, 0), (2, 0, 1, 3, 0),
+        (2, 0, 1, 0, 0),
     ),
     (
-        (0, 0, 2, 0, 0), (0, 0, 2, 1, 0), (0, 0, 2, 2, 0), (0, 0, 2, 3, 0), (1, 0, 2, 1, 2), (1, 0, 2, 2, 1),
-        (1, 0, 2, 2, 0), (1, 0, 2, 0, 2), (1, 0, 2, 3, 1), (1, 0, 2, 3, 0), (3, 0, 2, 0, 0), (1, 0, 2, 2, 2),
-        (1, 0, 2, 1, 1), (1, 0, 2, 0, 0), (3, 0, 2, 1, 0), (0, 0, 3, 0, 0), (0, 0, 1, 3, 0), (0, 1, 2, 2, 0),
-        (1, 0, 3, 0, 2), (1, 0, 1, 3, 0), (1, 0, 1, 3, 1), (0, 0, 1, 1, 0), (1, 1, 2, 2, 2), (0, 0, 3, 1, 0),
-        (1, 0, 3, 1, 0), (0, 1, 2, 3, 0), (1, 0, 1, 1, 1), (3, 0, 3, 0, 0), (0, 0, 3, 2, 0), (0, 0, 1, 0, 0),
-        (0, 1, 2, 0, 0), (1, 0, 3, 2, 2), (1, 0, 1, 0, 1), (1, 0, 2, 1, 0), (3, 1, 2, 1, 0), (0, 0, 3, 3, 0),
-        (0, 0, 0, 1, 0), (0, 1, 1, 3, 0), (1, 0, 0, 1, 0), (1, 0, 3, 3, 2), (1, 0, 0, 1, 1), (3, 0, 1, 0, 0),
-        (0, 0, 0, 0, 0), (0, 1, 3, 1, 0), (0, 1, 3, 2, 0), (1, 0, 0, 0, 0), (1, 1, 3, 1, 2), (1, 0, 0, 0, 1),
-        (3, 0, 3, 1, 0), (0, 0, 0, 2, 0), (0, 1, 2, 1, 0), (0, 1, 3, 3, 0), (1, 0, 0, 2, 1), (1, 0, 0, 2, 0),
-        (1, 0, 3, 1, 2), (3, 0, 0, 0, 0), (0, 0, 0, 3, 0), (0, 1, 0, 1, 0), (0, 1, 3, 0, 0), (1, 0, 0, 3, 1),
-        (1, 0, 2, 3, 2), (3, 1, 3, 1, 0), (0, 0, 1, 2, 0), (0, 1, 0, 0, 0), (1, 0, 1, 2, 0), (1, 1, 0, 1, 1),
-        (2, 1, 2, 3, 2), (3, 1, 2, 0, 0), (0, 1, 1, 1, 0), (0, 1, 0, 2, 0), (1, 1, 1, 1, 1), (3, 0, 1, 1, 0),
-        (0, 1, 1, 0, 0), (2, 1, 2, 1, 0), (1, 1, 1, 0, 1), (3, 1, 0, 0, 0), (0, 1, 1, 2, 0), (0, 1, 0, 3, 0),
-        (1, 1, 1, 2, 1), (3, 0, 0, 1, 0), (3, 1, 3, 0, 0), (2, 1, 0, 1, 2), (1, 0, 1, 2, 1), (2, 1, 2, 2, 0),
-        (3, 1, 1, 1, 0), (2, 1, 3, 1, 0), (1, 1, 2, 1, 1), (2, 0, 0, 0, 2), (3, 1, 1, 0, 0), (2, 1, 1, 3, 0),
-        (1, 1, 2, 0, 1), (3, 1, 0, 1, 0), (2, 1, 1, 1, 0), (2, 1, 1, 0, 1), (2, 0, 0, 3, 2), (2, 1, 3, 3, 1),
-        (2, 1, 0, 0, 2), (2, 1, 3, 2, 0), (1, 0, 2, 0, 1), (2, 1, 0, 2, 0), (2, 1, 0, 3, 2), (2, 1, 1, 2, 0),
-        (2, 1, 2, 0, 1), (2, 0, 0, 1, 2), (2, 1, 3, 0, 1), (2, 0, 0, 2, 2), (2, 0, 1, 1, 2), (2, 0, 3, 0, 1),
-        (2, 0, 1, 2, 2), (2, 0, 3, 1, 1), (2, 0, 1, 3, 2), (2, 0, 3, 3, 1), (2, 0, 1, 0, 2), (2, 0, 3, 2, 1),
-        (2, 0, 2, 1, 0), (2, 0, 2, 2, 0), (2, 0, 2, 0, 0), (2, 0, 2, 3, 0),
+        (0, 0, 2, 0, 0), (0, 0, 2, 1, 0), (0, 0, 2, 2, 0), (0, 0, 2, 3, 0), (1, 0, 2, 3, 1), (1, 0, 2, 1, 2),
+        (1, 0, 2, 0, 0), (1, 0, 2, 1, 1), (1, 0, 2, 0, 2), (1, 0, 2, 2, 0), (3, 0, 2, 0, 0), (1, 0, 2, 3, 2),
+        (1, 0, 2, 2, 1), (1, 0, 2, 3, 0), (3, 0, 2, 1, 0), (0, 0, 1, 0, 0), (0, 0, 3, 3, 0), (0, 1, 2, 0, 0),
+        (1, 0, 1, 0, 1), (1, 0, 3, 3, 2), (1, 0, 3, 3, 0), (0, 0, 1, 1, 0), (0, 0, 3, 2, 0), (0, 1, 2, 2, 0),
+        (1, 0, 3, 2, 2), (1, 0, 3, 2, 0), (1, 0, 2, 0, 1), (3, 0, 1, 0, 0), (0, 0, 3, 1, 0), (0, 0, 1, 3, 0),
+        (0, 1, 2, 3, 0), (1, 0, 1, 1, 0), (1, 0, 3, 1, 2), (1, 0, 1, 1, 1), (3, 0, 3, 1, 0), (0, 0, 0, 1, 0),
+        (0, 0, 3, 0, 0), (0, 1, 3, 3, 0), (1, 0, 0, 1, 1), (1, 0, 2, 2, 2), (1, 0, 0, 1, 0), (3, 1, 2, 1, 0),
+        (0, 0, 0, 3, 0), (0, 1, 3, 0, 0), (0, 1, 3, 2, 0), (1, 1, 3, 0, 2), (1, 0, 0, 3, 1), (1, 0, 0, 3, 0),
+        (3, 0, 3, 0, 0), (0, 0, 0, 2, 0), (0, 1, 1, 1, 0), (1, 0, 0, 2, 1), (1, 0, 0, 2, 0), (1, 1, 2, 0, 2),
+        (3, 1, 3, 1, 0), (0, 1, 0, 0, 0), (0, 1, 0, 1, 0), (1, 1, 0, 0, 1), (1, 1, 3, 2, 2), (1, 0, 3, 1, 0),
+        (3, 0, 0, 1, 0), (0, 0, 0, 0, 0), (0, 1, 0, 3, 0), (1, 1, 0, 3, 1), (2, 1, 2, 2, 0), (1, 0, 3, 0, 2),
+        (3, 1, 0, 0, 0), (0, 0, 1, 2, 0), (0, 1, 0, 2, 0), (1, 0, 1, 2, 1), (1, 0, 1, 2, 0), (3, 0, 0, 0, 0),
+        (0, 1, 1, 0, 0), (0, 1, 3, 1, 0), (0, 1, 2, 1, 0), (2, 1, 0, 0, 0), (1, 1, 1, 0, 2), (1, 0, 0, 0, 1),
+        (3, 1, 0, 1, 0), (0, 1, 1, 3, 0), (1, 1, 1, 3, 1), (2, 1, 3, 3, 2), (2, 1, 0, 1, 0), (3, 1, 3, 0, 0),
+        (0, 1, 1, 2, 0), (1, 1, 2, 3, 1), (2, 1, 0, 2, 0), (3, 0, 1, 1, 0), (2, 0, 1, 0, 2), (1, 0, 1, 3, 1),
+        (2, 1, 3, 1, 0), (3, 1, 2, 0, 0), (3, 1, 1, 0, 0), (2, 0, 0, 3, 2), (1, 1, 3, 1, 1), (2, 1, 2, 0, 0),
+        (3, 1, 1, 1, 0), (2, 1, 1, 1, 0), (2, 1, 1, 0, 2), (2, 1, 1, 2, 0), (2, 0, 3, 2, 1), (2, 1, 0, 3, 2),
+        (2, 1, 1, 3, 0), (2, 1, 2, 1, 1), (2, 0, 0, 1, 2), (2, 1, 2, 3, 0), (2, 0, 0, 0, 2), (2, 1, 3, 2, 1),
+        (2, 0, 0, 2, 2), (2, 1, 3, 0, 1), (2, 0, 1, 1, 2), (2, 0, 3, 3, 1), (2, 0, 1, 2, 2), (2, 0, 3, 0, 1),
+        (2, 0, 1, 3, 2), (2, 0, 3, 1, 1), (2, 0, 2, 2, 0), (2, 0, 2, 3, 0), (2, 0, 2, 1, 0), (2, 0, 2, 0, 0),
     ),
     (
-        (0, 0, 3, 0, 0), (0, 0, 3, 1, 0), (0, 0, 3, 2, 0), (0, 0, 3, 3, 0), (1, 0, 3, 0, 2), (1, 0, 3, 2, 0),
-        (1, 0, 3, 1, 2), (1, 0, 3, 1, 0), (3, 0, 3, 0, 0), (1, 0, 3, 3, 0), (1, 0, 3, 2, 2), (3, 0, 3, 1, 0),
-        (1, 0, 3, 3, 2), (1, 0, 3, 0, 0), (0, 0, 2, 2, 0), (0, 1, 3, 2, 0), (1, 1, 3, 2, 2), (1, 0, 2, 2, 0),
-        (0, 0, 2, 3, 0), (0, 1, 3, 1, 0), (3, 0, 2, 1, 0), (0, 1, 3, 3, 0), (0, 0, 2, 1, 0), (1, 0, 2, 3, 0),
-        (1, 1, 3, 3, 2), (0, 0, 1, 3, 0), (0, 1, 3, 0, 0), (1, 0, 1, 3, 0), (1, 1, 3, 0, 2), (3, 1, 3, 1, 0),
-        (0, 0, 1, 1, 0), (0, 1, 2, 2, 0), (2, 0, 2, 2, 2), (3, 1, 3, 0, 0), (0, 0, 1, 0, 0), (0, 1, 2, 3, 0),
-        (2, 1, 3, 2, 0), (3, 0, 1, 0, 0), (0, 0, 0, 1, 0), (0, 1, 1, 3, 0), (2, 1, 3, 1, 2), (3, 1, 2, 1, 0),
-        (0, 0, 0, 0, 0), (1, 0, 0, 0, 0), (0, 0, 0, 2, 0), (1, 0, 0, 2, 0), (3, 0, 0, 0, 0), (0, 0, 0, 3, 0),
-        (1, 0, 0, 3, 0), (2, 1, 2, 2, 2), (2, 1, 2, 3, 0), (0, 1, 0, 0, 0), (2, 0, 0, 0, 2), (0, 1, 0, 1, 0),
-        (3, 0, 0, 1, 0), (3, 1, 0, 0, 0), (0, 1, 0, 2, 0), (0, 1, 1, 1, 0), (2, 0, 0, 3, 2), (0, 1, 0, 3, 0),
-        (0, 1, 1, 0, 0), (2, 1, 0, 0, 2), (2, 1, 0, 1, 0), (3, 1, 0, 1, 0), (0, 1, 1, 2, 0), (2, 0, 2, 3, 2),
-        (3, 1, 1, 0, 0), (0, 0, 1, 2, 0), (2, 1, 0, 2, 0), (2, 1, 0, 3, 2), (3, 1, 1, 1, 0), (0, 1, 2, 1, 0),
-        (2, 1, 1, 1, 0), (2, 0, 0, 1, 2), (3, 0, 1, 1, 0), (0, 1, 2, 0, 0), (2, 1, 1, 2, 0), (2, 1, 1, 3, 0),
-        (2, 0, 0, 2, 2), (3, 1, 2, 0, 0), (2, 0, 1, 1, 2), (2, 1, 1, 0, 0), (2, 1, 3, 3, 0), (2, 0, 1, 2, 2),
-        (0, 0, 2, 0, 0), (2, 1, 2, 1, 0), (2, 0, 1, 3, 2), (3, 0, 2, 0, 0), (2, 1, 2, 0, 0), (2, 0, 1, 0, 2),
-        (2, 1, 3, 0, 0), (2, 0, 2, 1, 2), (2, 0, 2, 0, 2), (2, 0, 3, 1, 0), (2, 0, 3, 0, 0), (2, 0, 3, 3, 0),
-        (2, 0, 3, 2, 0),
+        (0, 0, 3, 0, 0), (0, 0, 3, 1, 0), (0, 0, 3, 2, 0), (0, 0, 3, 3, 0), (1, 0, 3, 3, 0), (1, 0, 3, 3, 2),
+        (1, 0, 3, 0, 0), (1, 0, 3, 2, 2), (3, 0, 3, 0, 0), (1, 0, 3, 1, 2), (1, 0, 3, 2, 0), (3, 0, 3, 1, 0),
+        (0, 0, 2, 3, 0), (0, 1, 3, 3, 0), (1, 0, 3, 0, 2), (0, 1, 3, 0, 0), (0, 0, 2, 1, 0), (1, 0, 2, 1, 0),
+        (1, 1, 3, 0, 2), (0, 0, 2, 2, 0), (0, 1, 3, 2, 0), (1, 0, 2, 2, 0), (3, 0, 2, 1, 0), (0, 0, 1, 0, 0),
+        (0, 1, 2, 1, 0), (1, 0, 1, 0, 0), (3, 1, 3, 1, 0), (0, 0, 2, 0, 0), (0, 1, 2, 2, 0), (1, 0, 2, 0, 0),
+        (0, 0, 1, 1, 0), (1, 0, 1, 1, 0), (3, 0, 2, 0, 0), (0, 1, 1, 0, 0), (0, 0, 0, 1, 0), (1, 0, 0, 1, 0),
+        (1, 1, 1, 0, 2), (3, 0, 1, 0, 0), (2, 1, 3, 3, 2), (0, 1, 2, 0, 0), (0, 0, 0, 3, 0), (2, 0, 2, 0, 2),
+        (3, 1, 2, 0, 0), (0, 0, 0, 2, 0), (0, 1, 1, 1, 0), (2, 0, 1, 0, 2), (1, 0, 0, 2, 0), (0, 1, 0, 1, 0),
+        (0, 1, 0, 0, 0), (3, 0, 0, 1, 0), (0, 1, 0, 3, 0), (2, 1, 2, 0, 2), (3, 1, 0, 0, 0), (2, 0, 0, 3, 2),
+        (0, 0, 1, 2, 0), (0, 1, 0, 2, 0), (1, 0, 1, 2, 0), (3, 1, 1, 0, 0), (2, 1, 0, 1, 0), (0, 0, 0, 0, 0),
+        (3, 1, 0, 1, 0), (2, 1, 1, 0, 2), (2, 1, 0, 0, 0), (3, 0, 0, 0, 0), (0, 1, 1, 2, 0), (0, 1, 1, 3, 0),
+        (2, 1, 0, 2, 0), (2, 1, 0, 3, 2), (0, 1, 2, 3, 0), (2, 1, 1, 1, 0), (2, 0, 0, 1, 2), (3, 1, 1, 1, 0),
+        (0, 0, 1, 3, 0), (2, 0, 0, 0, 2), (3, 1, 2, 1, 0), (0, 1, 3, 1, 0), (2, 1, 1, 2, 0), (2, 0, 0, 2, 2),
+        (3, 0, 1, 1, 0), (2, 1, 1, 3, 0), (3, 1, 3, 0, 0), (2, 1, 2, 3, 0), (2, 0, 1, 1, 2), (2, 0, 1, 2, 2),
+        (2, 1, 2, 2, 0), (2, 0, 1, 3, 2), (2, 1, 2, 1, 0), (2, 0, 2, 3, 2), (2, 1, 3, 1, 0), (2, 0, 2, 2, 2),
+        (2, 1, 3, 2, 0), (2, 0, 2, 1, 2), (2, 1, 3, 0, 0), (2, 0, 3, 3, 0), (2, 0, 3, 2, 0), (2, 0, 3, 1, 0),
+        (2, 0, 3, 0, 0),
     ),
 )
 

time: 48.5 us -> 47.3 us (0.975)
  the two profiles are of different devices: /device:TPU:18 before, /device:TPU:0 now
where the time goes in v5:
time: 47.3 us; the launch traced here: 47.1 us
  Pallas kernels  45.4 us (96%)
  local copies, waits for them, and re-layouts  1.67 us (4%)
    pallas_call x1, Pallas kernels, fused_body(): pl.pallas_call(functools.partial(kernel, n), out_shape=jax.ShapeDtypeStru...  45.4 us
    unnamed x1, local copies, waits for them, and re-layouts  1.67 us

profile of v5, /device:TPU:0, one launch (start us, length us, event | category | flops | bytes accessed | tf_op | source)
XLA Modules:
  0.0 47.1 jit_solution(638107724271479786)
XLA Ops:
  0.0 45.4 %shard_map.73 = bf16[128,1024]{1,0:T(8,128)(2,1)} custom-call(bf16[128,1024]{1,0:T(8,128)(2,1)} %tok_hbm.1, f32[1,1024]{1,0:T(1,128)} %bitcast.3, s32[2,512]{1,0:T(2,128)} %bitcast.4, f32[2,512]{1,0:T(2,128)} %bitcast.5, bf16[1,1024,896]{2,1,0:T(8,128)(2,1)} %gate_hbm.1, bf16[1,1024,896]{2,1,0:T(8,128)(2,1)} %up_hbm.1, bf16[1,896,1024]{2,1,0:T(8,128)(2,1)} %down_hbm.1), custom_call_target="tpu_custom_call" | custom-call | tf_op jit(solution)/shard_map/pallas_call | solution.py:439
  45.4 1.7 %copy.9 = bf16[128,1024]{1,0:T(8,128)(2,1)} copy(bf16[128,1024]{1,0:T(8,128)(2,1)} %shard_map.73) | data formatting | bytes 524288
